TPU v7x, 32 devices: a whole 2x2x4 slice. The times are simulated.
32 devices in a mesh: sp: 8 (over z, core), tp: 4 (over y, x).
Axes of the slice: x: 2, y: 2, z: 4, core: 2. Of those that a mesh axis runs over, the one named last changes fastest.
Arguments:
- queries: bfloat16 [2048, 2048], P('sp', 'tp'), may hold values from -6 to 6
- keys: bfloat16 [2048, 1024], P('sp', 'tp'), may hold values from -6 to 6
- values: bfloat16 [2048, 1024], P('sp', 'tp'), may hold values from -6 to 6
- sink_logit: float32 [32], P('tp'), may hold values from -1 to 6
- out_weight: bfloat16 [2048, 2048], P(None, 'tp'), may hold values from -0.125 to 0.125
- residual: bfloat16 [2048, 2048], P(('sp', 'tp')), may hold values from -1.796875 to 1.796875
- norm_gain: float32 [2048], replicated, may hold values from 0.1 to 1.9
- routes: int32 [2048, 2], P(('sp', 'tp')), may hold values from 0 to 7, all different within a row; in each aligned block of 64 rows (0 to 63, 64 to 127, ...) at most 32 rows name the same one
- route_weights: float32 [2048, 2], P(('sp', 'tp')), may hold values from 0.2 to 1
- gate_weight: bfloat16 [8, 2048, 5120], P('sp', None, 'tp'), may hold values from -0.125 to 0.125
- up_weight: bfloat16 [8, 2048, 5120], P('sp', None, 'tp'), may hold values from -0.125 to 0.125
- down_weight: bfloat16 [8, 5120, 2048], P('sp', 'tp'), may hold values from -0.078125 to 0.078125
Outputs:
- mixed: bfloat16 [2048, 2048], P(('sp', 'tp'))
Inputs may be any that keep to these rules, and one draw needn't show every extreme that they name: `routes`: each row names two different experts. Among the rows of one device no expert is named more than 32 times, and in every draw some expert is named exactly 32 times by the rows of some device.
All inputs are finite; a program needn't handle non-finite values.
Results may differ from a plain program's by a relative error of at most 0.018.
Values may be sent and summed in bfloat16 or wider, within the bound.
A program may use at most 64 MiB of HBM per device.

v0:
```python
import functools

import jax
import jax.numpy as jnp
from jax import lax
from jax.experimental import pallas as pl
from jax.experimental.pallas import tpu as pltpu
from jax.sharding import PartitionSpec as P

HEADS = 32
KV_HEADS = 16
HEAD = 64
WINDOW = 128


EPS = 1e-06
NEGATIVE = -1e30
MESH = pl.DeviceIdType.MESH


def plane():
    t = lax.axis_index("tp")
    tx = t + 1 - 2 * lax.rem(t, 2)
    ty = lax.rem(t + 2, 4)
    return t, tx, ty, 3 - t


def greet(devices):
    barrier = pltpu.get_barrier_semaphore()
    for device in devices:
        pl.semaphore_signal(barrier, inc=1, device_id=device, device_id_type=MESH)
    pl.semaphore_wait(barrier, len(devices))


def remote(src, dst, send, recv, device):
    return pltpu.make_async_remote_copy(
        src_ref=src,
        dst_ref=dst,
        send_sem=send,
        recv_sem=recv,
        device_id=device,
        device_id_type=MESH,
    )


def flipped(index, mask):
    result = index
    bit = 1
    while bit <= mask:
        if mask & bit:
            result = result + bit * (1 - 2 * lax.rem(index // bit, 2))
        bit *= 2
    return result


def expert_kernel(
    send_ref, gate_hbm, up_hbm, down_hbm, out_ref,
    gate, up, down, piece, hidden, part, bx1, by1, bx2, by2, acc, fin, load,
    zs, zr, xs, xr, ys, yr, xhs, xhr, yhs, yhr,
    x1s, x1r, y1s, y1r, x2s, x2r, y2s, y2r, zls, zlr, zhs, zhr,
):
    n, capacity, width = send_ref.shape
    s = lax.axis_index("sp")
    t, tx, ty, td = plane()
    half = capacity // 2
    low, high = pl.ds(0, half), pl.ds(half, half)
    x_dev, y_dev = (s, tx), (s, ty)
    loads = [
        pltpu.make_async_copy(source, target, load.at[k])
        for k, (source, target) in enumerate(((gate_hbm, gate), (up_hbm, up), (down_hbm, down)))
    ]
    for copy in loads:
        copy.start()
    greet([(flipped(s, m), t) for m in range(1, n)] + [x_dev, y_dev])
    copies = []

    def go(*args):
        copy = remote(*args)
        copy.start()
        copies.append(copy)
        return copy

    def total(a, b):
        return (a.astype(jnp.float32) + b.astype(jnp.float32)).astype(jnp.bfloat16)

    gray = [k ^ (k >> 1) for k in range(n // 2)]
    z_copies, full, halves, first, second, back = {}, {}, {}, {}, {}, []

    def members(q):
        return (2 * q, 2 * q + 1)

    def stage_a(q):
        for m in members(q):
            source = flipped(s, m)
            if m:
                z_copies[m].wait_recv()
            src = piece.at[t, source] if m else send_ref.at[source]
            full[m] = (
                go(src, piece.at[t, source], xs.at[m], xr.at[m], x_dev),
                go(src, piece.at[t, source], ys.at[m], yr.at[m], y_dev),
            )

    def stage_b(q):
        for m in members(q):
            source = flipped(s, m)
            full[m][0].wait_recv()
            block = piece.at[tx, source, low]
            to_y = go(block, block, yhs.at[m], yhr.at[m], y_dev)
            full[m][1].wait_recv()
            block = piece.at[ty, source, high]
            halves[m] = (to_y, go(block, block, xhs.at[m], xhr.at[m], x_dev))

    def compute(q):
        for m in members(q):
            for copy in halves[m]:
                copy.wait_recv()
        base = flipped(s // 2, q) * 2
        rows = 8 * capacity
        step = 256

        @pl.loop(0, gate.shape[1] // step)
        def _(k):
            columns = pl.ds(pl.multiple_of(k * step, step), step)
            x = piece[:, pl.ds(base, 2)].reshape(rows, width)
            g = jnp.dot(x, gate[:, columns], preferred_element_type=jnp.float32)
            u = jnp.dot(x, up[:, columns], preferred_element_type=jnp.float32)
            hidden[:, columns] = (jax.nn.silu(g) * u).astype(hidden.dtype)

        wide = 512

        @pl.loop(0, width // wide)
        def _(k):
            columns = pl.ds(pl.multiple_of(k * wide, wide), wide)
            share = jnp.dot(hidden[...], down[:, columns], preferred_element_type=jnp.float32)
            part[:, pl.ds(base, 2), :, columns] = share.astype(part.dtype).reshape(
                4, 2, capacity, wide
            )

    def begin(q):
        for m in members(q):
            owner = flipped(s, m)
            first[m] = (
                go(part.at[td, owner, low], bx1.at[m, 1], x1s.at[m, 1], x1r.at[m, 1], x_dev),
                go(part.at[td, owner, high], by1.at[m, 1], y1s.at[m, 1], y1r.at[m, 1], y_dev),
                go(part.at[tx, owner, low], bx1.at[m, 0], x1s.at[m, 0], x1r.at[m, 0], x_dev),
                go(part.at[ty, owner, high], by1.at[m, 0], y1s.at[m, 0], y1r.at[m, 0], y_dev),
            )

    def middle(q):
        for m in members(q):
            owner = flipped(s, m)
            first[m][0].wait_recv()
            acc[m, 0] = total(part[ty, owner, low], bx1[m, 1])
            to_y = go(acc.at[m, 0], by2.at[m], y2s.at[m], y2r.at[m], y_dev)
            first[m][1].wait_recv()
            acc[m, 1] = total(part[tx, owner, high], by1[m, 1])
            second[m] = (to_y, go(acc.at[m, 1], bx2.at[m], x2s.at[m], x2r.at[m], x_dev))

    def last(q):
        for m in members(q):
            owner = flipped(s, m)
            first[m][2].wait_recv()
            second[m][0].wait_recv()
            lower = total(
                part[t, owner, low].astype(jnp.float32) + bx1[m, 0].astype(jnp.float32), by2[m]
            )
            first[m][3].wait_recv()
            second[m][1].wait_recv()
            upper = total(
                part[t, owner, high].astype(jnp.float32) + by1[m, 0].astype(jnp.float32), bx2[m]
            )
            if m:
                away = (owner, t)
                fin[m, low] = lower
                back.append(go(fin.at[m, low], out_ref.at[s, low], zls.at[m], zlr.at[m], away))
                fin[m, high] = upper
                back.append(go(fin.at[m, high], out_ref.at[s, high], zhs.at[m], zhr.at[m], away))
            else:
                out_ref[s, low] = lower
                out_ref[s, high] = upper

    for q in gray:
        for m in members(q):
            if m:
                target = flipped(s, m)
                z_copies[m] = go(
                    send_ref.at[target], piece.at[t, s], zs.at[m], zr.at[m], (target, t)
                )
    stage_a(0)
    piece[t, s] = send_ref[s]
    order = gray[1:] + [0]
    count = len(gray)
    for k in range(count + 4):
        if k + 1 < count:
            stage_a(gray[k + 1])
        if k < count:
            stage_b(gray[k])
        if k == 2:
            for copy in loads:
                copy.wait()
        if 0 <= k - 2 < count:
            compute(order[k - 2])
            begin(order[k - 2])
        if 0 <= k - 3 < count:
            middle(order[k - 3])
        if 0 <= k - 4 < count:
            last(order[k - 4])
    for copy in back:
        copy.wait_recv()
    for copy in copies:
        copy.wait_send()


def experts(sending, gate_weight, up_weight, down_weight):
    n, capacity, width = sending.shape
    half = capacity // 2
    kind = sending.dtype
    one = pltpu.SemaphoreType.DMA((n,))
    two = pltpu.SemaphoreType.DMA((n, 2))
    anywhere = pl.BlockSpec(memory_space=pl.ANY)
    return pl.pallas_call(
        expert_kernel,
        out_shape=jax.ShapeDtypeStruct((n, capacity, width), kind),
        in_specs=[pl.BlockSpec(memory_space=pltpu.VMEM), anywhere, anywhere, anywhere],
        out_specs=pl.BlockSpec(memory_space=pltpu.VMEM),
        scratch_shapes=[
            pltpu.VMEM(gate_weight.shape, kind),
            pltpu.VMEM(up_weight.shape, kind),
            pltpu.VMEM(down_weight.shape, kind),
            pltpu.VMEM((4, n, capacity, width), kind),
            pltpu.VMEM((8 * capacity, gate_weight.shape[1]), kind),
            pltpu.VMEM((4, n, capacity, width), kind),
            pltpu.VMEM((n, 2, half, width), kind),
            pltpu.VMEM((n, 2, half, width), kind),
            pltpu.VMEM((n, half, width), kind),
            pltpu.VMEM((n, half, width), kind),
            pltpu.VMEM((n, 2, half, width), kind),
            pltpu.VMEM((n, capacity, width), kind),
            pltpu.SemaphoreType.DMA((3,)),
        ]
        + [one] * 10
        + [two] * 4
        + [one] * 8,
        compiler_params=pltpu.CompilerParams(
            collective_id=0, has_side_effects=True, vmem_limit_bytes=56 * 1024 * 1024
        ),
    )(sending, gate_weight, up_weight, down_weight)


def project_kernel(x_ref, w_ref, out_ref, buf, acc, cols, gs, gr, as_, ar):
    s = lax.axis_index("sp")
    t, tx, ty, td = plane()
    rows, depth = x_ref.shape
    half = rows // 2
    low, high = pl.ds(0, half), pl.ds(half, half)
    x_dev, y_dev, d_dev = (s, tx), (s, ty), (s, td)
    greet([x_dev, y_dev, d_dev])
    copies = []

    def go(*args):
        copy = remote(*args)
        copy.start()
        copies.append(copy)
        return copy

    def product(piece, owner, columns):
        weight = w_ref[pl.ds(pl.multiple_of(owner * depth, depth), depth), columns]
        return jnp.dot(piece, weight, preferred_element_type=jnp.float32)

    x_low = go(x_ref.at[low], buf.at[t, low], gs.at[0], gr.at[0], x_dev)
    y_high = go(x_ref.at[high], buf.at[t, high], gs.at[1], gr.at[1], y_dev)
    x_high = go(x_ref.at[high], buf.at[t, high], gs.at[2], gr.at[2], x_dev)
    y_low = go(x_ref.at[low], buf.at[t, low], gs.at[3], gr.at[3], y_dev)
    acc[...] = product(x_ref[...], t, slice(None))
    x_low.wait_recv()
    d_low = go(buf.at[tx, low], buf.at[tx, low], gs.at[4], gr.at[4], y_dev)
    y_high.wait_recv()
    d_high = go(buf.at[ty, high], buf.at[ty, high], gs.at[5], gr.at[5], x_dev)
    x_high.wait_recv()
    acc[...] += product(buf[tx], tx, slice(None))
    y_low.wait_recv()
    acc[...] += product(buf[ty], ty, slice(None))
    d_low.wait_recv()
    d_high.wait_recv()
    tiles = 2
    width = w_ref.shape[1] // tiles
    own = rows // 4
    arrivals = []
    for tile in range(tiles):
        columns = slice(tile * width, (tile + 1) * width)
        total = acc[:, columns] + product(buf[td], td, columns)
        cols[tile] = total.astype(cols.dtype)
        for k, (owner, device) in enumerate(((td, d_dev), (tx, x_dev), (ty, y_dev))):
            arrivals.append(
                go(
                    cols.at[tile, pl.ds(pl.multiple_of(owner * own, own), own)],
                    out_ref.at[tile, t],
                    as_.at[tile, k],
                    ar.at[tile, k],
                    device,
                )
            )
        out_ref[tile, t] = cols[tile, pl.ds(pl.multiple_of(t * own, own), own)]
    for copy in arrivals:
        copy.wait_recv()
    for copy in copies:
        copy.wait_send()


def project(attention, out_weight):
    rows, depth = attention.shape
    width = out_weight.shape[1]
    kind = attention.dtype
    out = pl.pallas_call(
        project_kernel,
        out_shape=jax.ShapeDtypeStruct((2, 4, rows // 4, width // 2), kind),
        in_specs=[pl.BlockSpec(memory_space=pltpu.VMEM)] * 2,
        out_specs=pl.BlockSpec(memory_space=pltpu.VMEM),
        scratch_shapes=[
            pltpu.VMEM((4, rows, depth), kind),
            pltpu.VMEM((rows, width), jnp.float32),
            pltpu.VMEM((2, rows, width // 2), kind),
            pltpu.SemaphoreType.DMA((6,)),
            pltpu.SemaphoreType.DMA((6,)),
            pltpu.SemaphoreType.DMA((2, 3)),
            pltpu.SemaphoreType.DMA((2, 3)),
        ],
        compiler_params=pltpu.CompilerParams(collective_id=2, has_side_effects=True),
    )(attention, out_weight)
    return out.transpose(2, 1, 0, 3).reshape(rows // 4, 4 * width)


def with_halo(block, sides, width):
    for axis, dim in sides:
        count = lax.axis_size(axis)
        forward = [(i, i + 1) for i in range(count - 1)]
        backward = [(target, source) for source, target in forward]
        low = lax.ppermute(
            lax.slice_in_dim(block, block.shape[dim] - width, None, axis=dim), axis, forward
        )
        high = lax.ppermute(lax.slice_in_dim(block, 0, width, axis=dim), axis, backward)
        block = jnp.concatenate([low, block, high], axis=dim)
    return block


def make_band(extended, length):
    blocks = length // WINDOW
    pieces = [
        lax.slice_in_dim(extended, offset * WINDOW, offset * WINDOW + length, axis=0).reshape(
            blocks, WINDOW, -1
        )
        for offset in range(3)
    ]
    return jnp.concatenate(pieces, axis=1)


def attend_local(queries, keys, values, sink_logit):
    length = queries.shape[0]
    groups = keys.shape[1] // HEAD
    repeat = HEADS // KV_HEADS
    blocks = length // WINDOW
    joined = jnp.concatenate([keys, values], axis=1)
    extended = with_halo(joined, (("sp", 0),), WINDOW)
    banded = make_band(extended, length)
    key_band = banded[..., : groups * HEAD].reshape(blocks, 3 * WINDOW, groups, HEAD)
    value_band = banded[..., groups * HEAD :].reshape(blocks, 3 * WINDOW, groups, HEAD)
    query_blocks = queries.reshape(blocks, WINDOW, groups, repeat, HEAD)
    scores = jnp.einsum(
        "nqgrd,nkgd->ngrqk", query_blocks, key_band, preferred_element_type=jnp.float32
    ) * HEAD ** (-0.5)
    near = jnp.abs(jnp.arange(WINDOW)[:, None] + WINDOW - jnp.arange(3 * WINDOW)[None, :]) <= WINDOW
    first_token = lax.axis_index("sp") * length
    key_pos = (
        first_token + (jnp.arange(blocks)[:, None] - 1) * WINDOW + jnp.arange(3 * WINDOW)[None, :]
    )
    inside = (key_pos >= 0) & (key_pos < length * lax.axis_size("sp"))
    valid = near[None, None, None, :, :] & inside[:, None, None, None, :]
    sinks = sink_logit.reshape(1, groups, repeat, 1, 1)
    masked = jnp.where(valid, scores, NEGATIVE)
    top = jnp.maximum(jnp.max(masked, axis=-1, keepdims=True), sinks)
    probs = jnp.exp(masked - top)
    denom = jnp.sum(probs, axis=-1, keepdims=True) + jnp.exp(sinks - top)
    weights = (probs / denom).astype(jnp.bfloat16)
    output = jnp.einsum(
        "ngrqk,nkgd->nqgrd", weights, value_band, preferred_element_type=jnp.float32
    )
    return output.astype(jnp.bfloat16).reshape(length, groups * repeat * HEAD)


def local(
    queries,
    keys,
    values,
    sink_logit,
    out_weight,
    residual,
    norm_gain,
    routes,
    route_weights,
    gate_weight,
    up_weight,
    down_weight,
):
    attention = attend_local(queries, keys, values, sink_logit)
    capacity = max(2, 4 * residual.shape[0] // lax.axis_size("sp"))
    in_plane = (
        lax.axis_size("tp") == 4
        and lax.axis_size("sp") == 8
        and capacity % 32 == 0
        and gate_weight.shape[2] % 256 == 0
    )
    if in_plane:
        projected = project(attention, out_weight)
    else:
        columns = jnp.dot(
            lax.all_gather(attention, "tp", axis=1, tiled=True),
            out_weight,
            preferred_element_type=jnp.float32,
        )
        projected = lax.all_to_all(
            columns.astype(jnp.bfloat16), "tp", split_axis=0, concat_axis=1, tiled=True
        )
    hidden_state = residual.astype(jnp.float32) + projected.astype(jnp.float32)
    inverse = lax.rsqrt(jnp.mean(hidden_state * hidden_state, axis=-1, keepdims=True) + EPS)
    normed = (hidden_state * inverse * norm_gain).astype(jnp.bfloat16)
    sp_count = lax.axis_size("sp")
    tok_rows = residual.shape[0]
    width = residual.shape[1]
    slot_total = sp_count * capacity
    expert_ids = routes.reshape(-1)
    onehot = (expert_ids[:, None] == jnp.arange(sp_count, dtype=jnp.int32)[None, :]).astype(
        jnp.int32
    )
    earlier = jnp.cumsum(onehot, axis=0) - onehot
    rank = jnp.sum(earlier * onehot, axis=1)
    slots = expert_ids * capacity + rank
    placing = (slots[:, None] == jnp.arange(slot_total, dtype=jnp.int32)[None, :]).astype(
        jnp.bfloat16
    )
    placing = placing.reshape(tok_rows, 2, slot_total)
    first_place = placing[:, 0]
    second_place = placing[:, 1]
    sending = jnp.einsum(
        "ts,td->sd", first_place + second_place, normed, preferred_element_type=jnp.float32
    )
    sending = sending.astype(jnp.bfloat16).reshape(sp_count, capacity, width)
    if in_plane:
        returned = experts(sending, gate_weight[0], up_weight[0], down_weight[0])
    else:
        piece = lax.all_gather(
            lax.all_to_all(sending, "sp", split_axis=0, concat_axis=0, tiled=True),
            "tp",
            axis=0,
            tiled=True,
        )
        flat = piece.reshape(-1, piece.shape[-1])
        gate = jnp.dot(flat, gate_weight[0], preferred_element_type=jnp.float32)
        upward = jnp.dot(flat, up_weight[0], preferred_element_type=jnp.float32)
        hidden = (jax.nn.silu(gate) * upward).astype(jnp.bfloat16)
        partial_value = jnp.dot(hidden, down_weight[0], preferred_element_type=jnp.float32)
        partial_value = partial_value.reshape(piece.shape[:-1] + (down_weight.shape[-1],))
        returned = lax.all_to_all(
            lax.psum_scatter(
                partial_value.astype(jnp.bfloat16), "tp", scatter_dimension=0, tiled=True
            ),
            "sp",
            split_axis=0,
            concat_axis=0,
            tiled=True,
        )
    gathered_back = returned.reshape(slot_total, width)
    first_pick = jnp.dot(first_place, gathered_back, preferred_element_type=jnp.float32)
    second_pick = jnp.dot(second_place, gathered_back, preferred_element_type=jnp.float32)
    mixture = route_weights[:, 0:1] * first_pick + route_weights[:, 1:2] * second_pick
    return (hidden_state + mixture).astype(jnp.bfloat16)


def solution(mesh):
    in_specs = (
        P("sp", "tp"),
        P("sp", "tp"),
        P("sp", "tp"),
        P("tp"),
        P(None, "tp"),
        P(("sp", "tp"), None),
        P(),
        P(("sp", "tp"), None),
        P(("sp", "tp"), None),
        P("sp", None, "tp"),
        P("sp", None, "tp"),
        P("sp", "tp", None),
    )
    out_specs = P(("sp", "tp"), None)
    return jax.shard_map(local, mesh=mesh, in_specs=in_specs, out_specs=out_specs, check_vma=False)
```

profile of v0, /device:TPU:0, one launch (start us, length us, event | category | flops | bytes accessed | tf_op | source)
XLA Modules:
  0.0 134.2 jit_solution(10517487567614891137)
XLA Ops:
  0.0 0.9 constant_dynamic-update-slice_fusion.1
  0.9 0.9 constant_dynamic-update-slice_fusion
  1.9 2.4 %collective-permute-start = (bf16[128,512]{1,0:T(8,128)(2,1)S(1)}, bf16[128,512]{1,0:T(8,128)(2,1)S(1)}, u32[]{:S(2)}, u32[]{:S(2)}) collective-permute-start(bf16[128,512]{1,0:T(8,128)(2,1)S(1)} %get-tuple-element.9), channel_id=1, source_target_pairs={{0,4},{4,8},{8,12},{12,16},{16,20},{20,24},{24,28},{1,5},{5,9},{9,... | collective-permute-start | bytes 393224 | tf_op jit(solution)/shard_map/ppermute | solution.py:338
  4.3 1.3 collective-permute-start.1
  5.6 0.2 copy.36
  5.8 0.1 compare_and_fusion
  5.9 0.1 abs_compare_fusion
  5.9 1.3 reshape.158
  7.2 0.7 max.18
  7.9 0.8 copy.44
  8.7 0.1 eq.30
  8.8 0.1 fusion.12
  8.9 0.2 reduce_window_sum.11
  9.1 0.2 select_reduce_fusion
  9.3 0.1 reduce_sum.31
  9.4 0.1 copy.45
  9.5 0.7 multiply_add_fusion
  10.2 0.1 iota_compare_fusion
  10.3 0.2 broadcast_and_fusion
  10.5 0.8 slice_bitcast_fusion.4
  11.2 0.0 collective-permute-done
  11.2 0.0 collective-permute-done.1
  11.3 0.2 copy.37
  11.5 0.2 copy.35
  11.6 0.1 pad_maximum_fusion
  11.8 0.1 fusion.19
  11.8 0.7 fusion.1
  12.6 0.1 broadcast_maximum_fusion
  12.6 0.7 fusion
  13.3 0.1 exponential_add_fusion
  13.4 1.0 fusion.7
  14.3 0.4 copy.51
  14.8 0.0 copy-start
  14.8 1.0 reshape.159.x_ref
  15.8 0.0 copy-start.1
  15.8 20.4 %shard_map.118 = bf16[2,4,64,256]{3,2,1,0:T(8,128)(2,1)} custom-call(bf16[256,512]{1,0:T(8,128)(2,1)} %reshape.159.x_ref, bf16[2048,512]{1,0:T(8,128)(2,1)} %w_ref.1), custom_call_target="tpu_custom_call" | custom-call | tf_op jit(solution)/shard_map/pallas_call | solution.py:314
  36.2 1.0 convert_bitcast_fusion
  37.2 0.4 copy.43
  37.6 0.4 reshape.155
  38.0 0.0 copy-done
  38.0 0.2 multiply_reduce_fusion
  38.2 0.0 copy-done.1
  38.2 1.5 %convolution_convert_fusion = bf16[256,2048]{1,0:T(8,128)(2,1)} fusion(f32[2048]{0:T(1024)S(1)} %copy-done.1, f32[64]{0:T(128)S(1)} %add_rsqrt_fusion, f32[64,2048]{1,0:T(8,128)S(1)} %reshape.155, bf16[64,2048]{1,0:T(8,128)(2,1)S(1)} %copy-done, bf16[64,2,256]{2,0,1:T(8,128)(2,1)S(1)} %get-tuple-element.14), kind=kOutput, calls=%fused_computation.4 | convolution fusion | flops 68304896 | bytes 1908992 | tf_op jit(solution)/shard_map/ts,td->sd/dot_general | solution.py:443
  39.7 90.8 %shard_map.119 = bf16[8,32,2048]{2,1,0:T(8,128)(2,1)} custom-call(bf16[8,32,2048]{2,1,0:T(8,128)(2,1)} %bitcast.57, bf16[2048,1280]{1,0:T(8,128)(2,1)} %bitcast.54, bf16[2048,1280]{1,0:T(8,128)(2,1)} %bitcast.55, bf16[1280,2048]{1,0:T(8,128)(2,1)} %bitcast.56), custom_call_target="tpu_custom_call" | custom-call | tf_op jit(solution)/shard_map/pallas_call | solution.py:221
  130.5 1.5 %convolution_multiply_fusion.1 = f32[64,2048]{1,0:T(8,128)S(1)} fusion(bf16[256,2048]{1,0:T(8,128)(2,1)} %bitcast.52, f32[64]{0:T(128)S(1)} %get-tuple-element.12, pred[64,2,256]{2,0,1:T(32,128)(4,1)S(1)} %get-tuple-element.13), kind=kOutput, calls=%fused_computation.8 | convolution fusion | flops 67239936 | bytes 1589760 | tf_op jit(solution)/shard_map/dot_general | solution.py:472
  132.0 2.2 %fusion.4 = bf16[64,2048]{1,0:T(8,128)(2,1)} fusion(f32[64,2048]{1,0:T(8,128)S(1)} %convolution_multiply_fusion.1, bf16[256,2048]{1,0:T(8,128)(2,1)} %bitcast.53, f32[64]{0:T(128)S(1)} %get-tuple-element.11, f32[64,2048]{1,0:T(8,128)S(1)} %reshape.155, bf16[64,2048]{1,0:T(8,128)(2,1)S(1)} %copy-done, pred[64,2,256]{2,0,1:T(32,128)(4,1)S(1)} %get-tuple-element.13), kind=kOutput, calls=%fused_computation.10 | convolution fusion | flops 67895296 | bytes 2638336 | tf_op jit(solution)/shard_map/dot_general | solution.py:473
  (5 shorter events, 0.1 us)
Async XLA Ops:
  1.9 9.4 %collective-permute-start = (bf16[128,512]{1,0:T(8,128)(2,1)S(1)}, bf16[128,512]{1,0:T(8,128)(2,1)S(1)}, u32[]{:S(2)}, u32[]{:S(2)}) collective-permute-start(bf16[128,512]{1,0:T(8,128)(2,1)S(1)} %get-tuple-element.9), channel_id=1, source_target_pairs={{0,4},{4,8},{8,12},{12,16},{16,20},{20,24},{24,28},{1,5},{5,9},{9,... | collective-permute-start | bytes 393224 | tf_op jit(solution)/shard_map/ppermute | solution.py:338
  4.3 7.0 %collective-permute-start.1 = (bf16[128,512]{1,0:T(8,128)(2,1)S(1)}, bf16[128,512]{1,0:T(8,128)(2,1)S(1)}, u32[]{:S(2)}, u32[]{:S(2)}) collective-permute-start(bf16[128,512]{1,0:T(8,128)(2,1)S(1)} %get-tuple-element.10), channel_id=1, source_target_pairs={{4,0},{8,4},{12,8},{16,12},{20,16},{24,20},{28,24},{5,1},{9,5},{13... | collective-permute-start | bytes 393224 | tf_op jit(solution)/shard_map/ppermute | solution.py:341
  14.8 23.2 %copy-start = (bf16[64,2048]{1,0:T(8,128)(2,1)S(1)}, bf16[64,2048]{1,0:T(8,128)(2,1)}, u32[]{:S(2)}) copy-start(bf16[64,2048]{1,0:T(8,128)(2,1)} %param.17) | copy-start | bytes 786436
  15.8 22.4 %copy-start.1 = (f32[2048]{0:T(1024)S(1)}, f32[2048]{0:T(1024)}, u32[]{:S(2)}) copy-start(f32[2048]{0:T(1024)} %param.18) | copy-start | bytes 24580
where the time goes:
time: 135 us; the launch traced here: 134 us
  Pallas kernels  111 us (82%)
  local copies, waits for them, and re-layouts  8.59 us (6%)
  matrix products  6.91 us (5%)
  starting transfers between devices  3.7 us (3%)
  other arithmetic  3.67 us (3%)
    pallas_call x1, Pallas kernels, experts(): pl.pallas_call(expert_kernel, out_shape=jax.ShapeDtypeStruct((n, capacity...  90.8 us
    pallas_call x1, Pallas kernels, project(): pl.pallas_call(project_kernel, out_shape=jax.ShapeDtypeStruct((2, 4, rows...  20.4 us
  transfers between devices with their start and end apart: 2, of which 0 were waited for; matrix products, arithmetic and copies ran while one was open for 4% of the time, Pallas kernels for 0%

commit v1 on v0

--- a/solution.py
+++ b/solution.py
@@ -247,14 +247,115 @@
     )(sending, gate_weight, up_weight, down_weight)
 
 
-def project_kernel(x_ref, w_ref, out_ref, buf, acc, cols, gs, gr, as_, ar):
+def attend_kernel(
+    q_hbm, k_hbm, v_hbm, sink_ref, w_hbm, res_hbm, gain_ref, hidden_ref, normed_ref,
+    q, kv, w, res, buf, acc, cols, got,
+    load, hs, hr, gs, gr, as_, ar,
+):
     s = lax.axis_index("sp")
     t, tx, ty, td = plane()
-    rows, depth = x_ref.shape
+    last = lax.axis_size("sp") - 1
+    rows, depth = q.shape
     half = rows // 2
-    low, high = pl.ds(0, half), pl.ds(half, half)
-    x_dev, y_dev, d_dev = (s, tx), (s, ty), (s, td)
-    greet([x_dev, y_dev, d_dev])
+    groups = k_hbm.shape[1] // HEAD
+    kept = groups * HEAD
+    odd = lax.rem(s, 2)
+    near = s + 1 - 2 * odd
+    has_far = jnp.logical_and(s != 0, s != last)
+    far = jnp.where(has_far, s - 1 + 2 * odd, near)
+    x_dev, y_dev, d_dev, n_dev, f_dev = (s, tx), (s, ty), (s, td), (near, t), (far, t)
+    middle = pl.ds(half, rows)
+    loads = [
+        pltpu.make_async_copy(source, target, load.at[k])
+        for k, (source, target) in enumerate(
+            (
+                (k_hbm, kv.at[middle, pl.ds(0, kept)]),
+                (v_hbm, kv.at[middle, pl.ds(kept, kept)]),
+                (q_hbm, q),
+                (w_hbm, w),
+                (res_hbm, res),
+            )
+        )
+    ]
+    for copy in loads:
+        copy.start()
+    barrier = pltpu.get_barrier_semaphore()
+    for device in (x_dev, y_dev, d_dev, n_dev):
+        pl.semaphore_signal(barrier, inc=1, device_id=device, device_id_type=MESH)
+
+    @pl.when(has_far)
+    def _():
+        pl.semaphore_signal(barrier, inc=1, device_id=f_dev, device_id_type=MESH)
+        pl.semaphore_wait(barrier, 5)
+
+    @pl.when(jnp.logical_not(has_far))
+    def _():
+        pl.semaphore_wait(barrier, 4)
+
+    def aligned(value, size):
+        return pl.ds(pl.multiple_of(value, size), size)
+
+    near_src = aligned(2 * half - half * odd, half)
+    near_dst = aligned(3 * half * odd, half)
+    far_src = aligned(half + half * odd, half)
+    far_dst = aligned(3 * half * (1 - odd), half)
+    near_copy = remote(kv.at[near_src], kv.at[near_dst], hs.at[0], hr.at[0], n_dev)
+    far_copy = remote(kv.at[far_src], kv.at[far_dst], hs.at[1], hr.at[1], f_dev)
+    loads[0].wait()
+    loads[1].wait()
+
+    @pl.when(has_far)
+    def _():
+        far_copy.start()
+
+    near_copy.start()
+
+    @pl.when(jnp.logical_not(has_far))
+    def _():
+        kv[aligned(3 * half * odd, half)] = jnp.zeros((half, kv.shape[1]), kv.dtype)
+
+    loads[2].wait()
+    span = 3 * half
+    query = lax.broadcasted_iota(jnp.int32, (2 * half, span), 0)
+    query = jnp.where(query >= half, query - half, query)
+    key = lax.broadcasted_iota(jnp.int32, (2 * half, span), 1)
+    band = jnp.abs(query + half - key) <= WINDOW
+    upper = lax.broadcasted_iota(jnp.int32, (2 * half, 1), 0) < half
+
+    def attend(b):
+        valid = jnp.logical_and(
+            band,
+            jnp.logical_and(
+                key >= jnp.where(2 * s + b == 0, half, 0),
+                key < jnp.where(2 * s + b == 2 * last + 1, 2 * half, span),
+            ),
+        )
+        keys_at = pl.ds(pl.multiple_of(b * half, half), span)
+        mine = aligned(b * half, half)
+        for g in range(groups):
+            pair = q[mine, 2 * g * HEAD : 2 * (g + 1) * HEAD]
+            stacked = jnp.concatenate([pair[:, :HEAD], pair[:, HEAD:]], axis=0)
+            scores = lax.dot_general(
+                stacked,
+                kv[keys_at, g * HEAD : (g + 1) * HEAD],
+                (((1,), (1,)), ((), ())),
+                preferred_element_type=jnp.float32,
+            ) * HEAD ** (-0.5)
+            sink = jnp.where(upper, sink_ref[2 * g], sink_ref[2 * g + 1])
+            masked = jnp.where(valid, scores, NEGATIVE)
+            top = jnp.maximum(jnp.max(masked, axis=-1, keepdims=True), sink)
+            probs = jnp.exp(masked - top)
+            denom = jnp.sum(probs, axis=-1, keepdims=True) + jnp.exp(sink - top)
+            weights = (probs * (1.0 / denom)).astype(jnp.bfloat16)
+            output = jnp.dot(
+                weights,
+                kv[keys_at, kept + g * HEAD : kept + (g + 1) * HEAD],
+                preferred_element_type=jnp.float32,
+            )
+            joined = jnp.concatenate([output[:half], output[half:]], axis=1)
+            buf[t, mine, 2 * g * HEAD : 2 * (g + 1) * HEAD] = joined.astype(buf.dtype)
+
+    first_block, second_block = 1 - odd, odd
     copies = []
 
     def go(*args):
@@ -263,71 +364,138 @@
         copies.append(copy)
         return copy
 
-    def product(piece, owner, columns):
-        weight = w_ref[pl.ds(pl.multiple_of(owner * depth, depth), depth), columns]
+    def spread(b, k):
+        piece = buf.at[t, aligned(b * half, half)]
+        return (
+            go(piece, piece, gs.at[k], gr.at[k], x_dev),
+            go(piece, piece, gs.at[k + 1], gr.at[k + 1], y_dev),
+        )
+
+    near_copy.wait_recv()
+    attend(first_block)
+    x_one, y_one = spread(first_block, 0)
+
+    @pl.when(has_far)
+    def _():
+        far_copy.wait_recv()
+
+    attend(second_block)
+    x_two, y_two = spread(second_block, 2)
+    loads[3].wait()
+
+    def product(b, owner):
+        weight = w[pl.ds(pl.multiple_of(owner * depth, depth), depth)]
+        piece = buf[owner, aligned(b * half, half)]
         return jnp.dot(piece, weight, preferred_element_type=jnp.float32)
 
-    x_low = go(x_ref.at[low], buf.at[t, low], gs.at[0], gr.at[0], x_dev)
-    y_high = go(x_ref.at[high], buf.at[t, high], gs.at[1], gr.at[1], y_dev)
-    x_high = go(x_ref.at[high], buf.at[t, high], gs.at[2], gr.at[2], x_dev)
-    y_low = go(x_ref.at[low], buf.at[t, low], gs.at[3], gr.at[3], y_dev)
-    acc[...] = product(x_ref[...], t, slice(None))
-    x_low.wait_recv()
-    d_low = go(buf.at[tx, low], buf.at[tx, low], gs.at[4], gr.at[4], y_dev)
-    y_high.wait_recv()
-    d_high = go(buf.at[ty, high], buf.at[ty, high], gs.at[5], gr.at[5], x_dev)
-    x_high.wait_recv()
-    acc[...] += product(buf[tx], tx, slice(None))
-    y_low.wait_recv()
-    acc[...] += product(buf[ty], ty, slice(None))
-    d_low.wait_recv()
-    d_high.wait_recv()
-    tiles = 2
-    width = w_ref.shape[1] // tiles
+    x_one.wait_recv()
+    piece = buf.at[tx, aligned(first_block * half, half)]
+    d_one = go(piece, piece, gs.at[4], gr.at[4], y_dev)
+    acc[0] = product(first_block, t)
+    acc[0] += product(first_block, tx)
+    y_one.wait_recv()
+    acc[0] += product(first_block, ty)
+    y_two.wait_recv()
+    piece = buf.at[ty, aligned(second_block * half, half)]
+    d_two = go(piece, piece, gs.at[5], gr.at[5], x_dev)
+    acc[1] = product(second_block, t)
+    acc[1] += product(second_block, ty)
     own = rows // 4
-    arrivals = []
-    for tile in range(tiles):
-        columns = slice(tile * width, (tile + 1) * width)
-        total = acc[:, columns] + product(buf[td], td, columns)
-        cols[tile] = total.astype(cols.dtype)
-        for k, (owner, device) in enumerate(((td, d_dev), (tx, x_dev), (ty, y_dev))):
-            arrivals.append(
-                go(
-                    cols.at[tile, pl.ds(pl.multiple_of(owner * own, own), own)],
-                    out_ref.at[tile, t],
-                    as_.at[tile, k],
-                    ar.at[tile, k],
-                    device,
-                )
-            )
-        out_ref[tile, t] = cols[tile, pl.ds(pl.multiple_of(t * own, own), own)]
-    for copy in arrivals:
-        copy.wait_recv()
+    to_x = remote(
+        cols.at[aligned(tx * own, own)], got.at[t], as_.at[0], ar.at[0], x_dev
+    )
+    to_y = remote(
+        cols.at[aligned(ty * own, own)], got.at[t], as_.at[1], ar.at[1], y_dev
+    )
+    to_d = remote(
+        cols.at[aligned(td * own, own)], got.at[t], as_.at[2], ar.at[2], d_dev
+    )
+    home = t // 2
+
+    def finish(b, k):
+        total = acc[k] + product(b, td)
+        cols[aligned(b * half, half)] = total.astype(cols.dtype)
+
+        @pl.when(home == b)
+        def _():
+            to_x.start()
+
+        @pl.when(home != b)
+        def _():
+            to_d.start()
+            to_y.start()
+
+    d_one.wait_recv()
+    finish(first_block, 0)
+    x_two.wait_recv()
+    acc[1] += product(second_block, tx)
+    d_two.wait_recv()
+    finish(second_block, 1)
+    got[t] = cols[aligned(t * own, own)]
+    loads[4].wait()
+    to_x.wait_recv()
+    to_y.wait_recv()
+    to_d.wait_recv()
+    squares = jnp.zeros((own, 1), jnp.float32)
+    width = w.shape[1]
+    for k in range(4):
+        columns = slice(k * width, (k + 1) * width)
+        state = res[:, columns].astype(jnp.float32) + got[k].astype(jnp.float32)
+        hidden_ref[:, columns] = state
+        squares += jnp.sum(state * state, axis=-1, keepdims=True)
+    inverse = lax.rsqrt(squares * (1.0 / (4 * width)) + EPS)
+    for k in range(4):
+        columns = slice(k * width, (k + 1) * width)
+        normed_ref[:, columns] = (
+            hidden_ref[:, columns] * inverse * gain_ref[:, columns]
+        ).astype(normed_ref.dtype)
     for copy in copies:
         copy.wait_send()
-
-
-def project(attention, out_weight):
-    rows, depth = attention.shape
+    near_copy.wait_send()
+    to_x.wait_send()
+    to_y.wait_send()
+    to_d.wait_send()
+
+    @pl.when(has_far)
+    def _():
+        far_copy.wait_send()
+
+
+def attend_project(queries, keys, values, sink_logit, out_weight, residual, norm_gain):
+    rows, depth = queries.shape
+    kind = queries.dtype
     width = out_weight.shape[1]
-    kind = attention.dtype
-    out = pl.pallas_call(
-        project_kernel,
-        out_shape=jax.ShapeDtypeStruct((2, 4, rows // 4, width // 2), kind),
-        in_specs=[pl.BlockSpec(memory_space=pltpu.VMEM)] * 2,
-        out_specs=pl.BlockSpec(memory_space=pltpu.VMEM),
+    anywhere = pl.BlockSpec(memory_space=pl.ANY)
+    vmem = pl.BlockSpec(memory_space=pltpu.VMEM)
+    dma = pltpu.SemaphoreType.DMA
+    return pl.pallas_call(
+        attend_kernel,
+        out_shape=(
+            jax.ShapeDtypeStruct(residual.shape, jnp.float32),
+            jax.ShapeDtypeStruct(residual.shape, kind),
+        ),
+        in_specs=[anywhere] * 3
+        + [pl.BlockSpec(memory_space=pltpu.SMEM), anywhere, anywhere, vmem],
+        out_specs=(vmem, vmem),
         scratch_shapes=[
+            pltpu.VMEM(queries.shape, kind),
+            pltpu.VMEM((2 * rows, 2 * keys.shape[1]), kind),
+            pltpu.VMEM(out_weight.shape, kind),
+            pltpu.VMEM(residual.shape, kind),
             pltpu.VMEM((4, rows, depth), kind),
-            pltpu.VMEM((rows, width), jnp.float32),
-            pltpu.VMEM((2, rows, width // 2), kind),
-            pltpu.SemaphoreType.DMA((6,)),
-            pltpu.SemaphoreType.DMA((6,)),
-            pltpu.SemaphoreType.DMA((2, 3)),
-            pltpu.SemaphoreType.DMA((2, 3)),
+            pltpu.VMEM((2, rows // 2, width), jnp.float32),
+            pltpu.VMEM((rows, width), kind),
+            pltpu.VMEM((4, rows // 4, width), kind),
+            dma((5,)),
+            dma((2,)),
+            dma((2,)),
+            dma((6,)),
+            dma((6,)),
+            dma((3,)),
+            dma((3,)),
         ],
         compiler_params=pltpu.CompilerParams(collective_id=2, has_side_effects=True),
-    )(attention, out_weight)
-    return out.transpose(2, 1, 0, 3).reshape(rows // 4, 4 * width)
+    )(queries, keys, values, sink_logit, out_weight, residual, norm_gain.reshape(1, -1))
 
 
 def with_halo(block, sides, width):
@@ -401,17 +569,20 @@
     up_weight,
     down_weight,
 ):
-    attention = attend_local(queries, keys, values, sink_logit)
     capacity = max(2, 4 * residual.shape[0] // lax.axis_size("sp"))
     in_plane = (
         lax.axis_size("tp") == 4
         and lax.axis_size("sp") == 8
         and capacity % 32 == 0
         and gate_weight.shape[2] % 256 == 0
+        and queries.shape[0] == 2 * WINDOW
     )
     if in_plane:
-        projected = project(attention, out_weight)
+        hidden_state, normed = attend_project(
+            queries, keys, values, sink_logit, out_weight, residual, norm_gain
+        )
     else:
+        attention = attend_local(queries, keys, values, sink_logit)
         columns = jnp.dot(
             lax.all_gather(attention, "tp", axis=1, tiled=True),
             out_weight,
@@ -420,9 +591,9 @@
         projected = lax.all_to_all(
             columns.astype(jnp.bfloat16), "tp", split_axis=0, concat_axis=1, tiled=True
         )
-    hidden_state = residual.astype(jnp.float32) + projected.astype(jnp.float32)
-    inverse = lax.rsqrt(jnp.mean(hidden_state * hidden_state, axis=-1, keepdims=True) + EPS)
-    normed = (hidden_state * inverse * norm_gain).astype(jnp.bfloat16)
+        hidden_state = residual.astype(jnp.float32) + projected.astype(jnp.float32)
+        inverse = lax.rsqrt(jnp.mean(hidden_state * hidden_state, axis=-1, keepdims=True) + EPS)
+        normed = (hidden_state * inverse * norm_gain).astype(jnp.bfloat16)
     sp_count = lax.axis_size("sp")
     tok_rows = residual.shape[0]
     width = residual.shape[1]

time: 135 us -> 123 us (0.911)
  local copies, waits for them, and re-layouts: 8.59 us -> 1.13 us
  starting transfers between devices: 3.7 us -> 0 us
  Pallas kernels: 111 us -> 114 us
  other arithmetic: 3.67 us -> 1.22 us
    pallas_call x1, Pallas kernels: 20.4 us -> 25.5 us  [attend_project(): pl.pallas_call(attend_kernel, out_shape=(jax.ShapeDtypeStruct(residual.sh...]
    ppermute x2 -> x0, starting transfers between devices: 3.7 us -> none  [the longest x1 2.4 us: with_halo(): lax.ppermute(lax.slice_in_dim(block, block.shape[dim] - width, None, axis...]
    reshape x6 -> x0, local copies, waits for them, and re-layouts: 3.21 us -> none  [the longest x2 1.43 us: attend_local(): return output.astype(jnp.bfloat16).reshape(length, groups * repeat * HEAD)]
    pallas_call x1, Pallas kernels: 90.8 us -> 88.2 us  [experts(): pl.pallas_call(expert_kernel, out_shape=jax.ShapeDtypeStruct((n, capacity...]
    dot_general x2 -> x0, matrix products: 1.66 us -> none  [the longest x1 0.95 us: attend_local(): jnp.einsum('ngrqk,nkgd->nqgrd', weights, value_band, preferred_element_ty...]
  transfers between devices with their start and end apart: 2 -> 0, of which waited for: 0 -> 0; matrix products, arithmetic and copies ran while one was open for 4% -> 0% of each run, Pallas kernels for 0% -> 0%
where the time goes in v1:
time: 123 us; the launch traced here: 122 us
  Pallas kernels  114 us (93%)
  matrix products  6.16 us (5%)
    pallas_call x1, Pallas kernels, experts(): pl.pallas_call(expert_kernel, out_shape=jax.ShapeDtypeStruct((n, capacity...  88.2 us
    pallas_call x1, Pallas kernels, attend_project(): pl.pallas_call(attend_kernel, out_shape=(jax.ShapeDtypeStruct(residual.sh...  25.5 us

profile of v1, /device:TPU:0, one launch (start us, length us, event | category | flops | bytes accessed | tf_op | source)
XLA Modules:
  0.0 122.3 jit_solution(7140517516280076260)
XLA Ops:
  0.0 25.5 %shard_map.118 = (f32[64,2048]{1,0:T(8,128)}, bf16[64,2048]{1,0:T(8,128)(2,1)}) custom-call(bf16[256,512]{1,0:T(8,128)(2,1)} %q_hbm.1, bf16[256,256]{1,0:T(8,128)(2,1)} %k_hbm.1, bf16[256,256]{1,0:T(8,128)(2,1)} %v_hbm.1, f32[8]{0:T(128)} %sink_ref.1, bf16[2048,512]{1,0:T(8,128)(2,1)} %w_hbm.1, bf16[64,2048]{1,0:T(8,128)(2,1)} %res_hbm.1, f32[1,2048]{1,0:T(1,128)} %bitcast.28), custom_call_target="tpu_custom_call" | custom-call | tf_op jit(solution)/shard_map/pallas_call | solution.py:471
  25.5 0.8 copy.20
  26.2 0.1 eq.30
  26.4 0.1 fusion.3
  26.5 0.2 reduce_window_sum.11
  26.6 0.2 select_reduce_fusion
  26.8 0.1 reduce_sum.12
  27.0 0.1 copy.21
  27.0 0.7 multiply_add_fusion
  27.7 0.1 iota_compare_fusion
  27.8 2.4 %convolution_convert_fusion = bf16[256,2048]{1,0:T(8,128)(2,1)} fusion(bf16[64,2048]{1,0:T(8,128)(2,1)} %get-tuple-element.8, bf16[64,2,256]{2,0,1:T(8,128)(2,1)S(1)} %get-tuple-element.12), kind=kOutput, calls=%fused_computation | convolution fusion | flops 67649536 | bytes 1376256 | tf_op jit(solution)/shard_map/ts,td->sd/dot_general | solution.py:614
  30.2 0.0 copy-start.1
  30.2 0.0 copy-start
  30.2 88.2 %shard_map.119 = bf16[8,32,2048]{2,1,0:T(8,128)(2,1)} custom-call(bf16[8,32,2048]{2,1,0:T(8,128)(2,1)} %bitcast.27, bf16[2048,1280]{1,0:T(8,128)(2,1)} %bitcast.24, bf16[2048,1280]{1,0:T(8,128)(2,1)} %bitcast.25, bf16[1280,2048]{1,0:T(8,128)(2,1)} %bitcast.26), custom_call_target="tpu_custom_call" | custom-call | tf_op jit(solution)/shard_map/pallas_call | solution.py:221
  118.5 0.0 copy-done.1
  118.5 1.5 %convolution_multiply_fusion.1 = f32[64,2048]{1,0:T(8,128)S(1)} fusion(bf16[256,2048]{1,0:T(8,128)(2,1)} %bitcast.22, f32[64]{0:T(128)S(1)} %get-tuple-element.10, pred[64,2,256]{2,0,1:T(32,128)(4,1)S(1)} %get-tuple-element.11), kind=kOutput, calls=%fused_computation.3 | convolution fusion | flops 67239936 | bytes 1589760 | tf_op jit(solution)/shard_map/dot_general | solution.py:643
  120.0 0.0 copy-done
  120.0 2.2 %fusion.2 = bf16[64,2048]{1,0:T(8,128)(2,1)} fusion(f32[64,2048]{1,0:T(8,128)S(1)} %copy-done, f32[64,2048]{1,0:T(8,128)S(1)} %convolution_multiply_fusion.1, bf16[256,2048]{1,0:T(8,128)(2,1)} %bitcast.23, f32[64]{0:T(128)S(1)} %get-tuple-element.9, pred[64,2,256]{2,0,1:T(32,128)(4,1)S(1)} %get-tuple-element.11), kind=kOutput, calls=%fused_computation.5 | convolution fusion | flops 67633152 | bytes 2376192 | tf_op jit(solution)/shard_map/dot_general | solution.py:644
  (1 shorter events, 0.0 us)
Async XLA Ops:
  30.2 88.2 %copy-start.1 = (f32[64,2]{0,1:T(2,128)S(1)}, f32[64,2]{0,1:T(2,128)}, u32[]{:S(2)}) copy-start(f32[64,2]{0,1:T(2,128)} %param.20) | copy-start | bytes 1540
  30.2 89.8 %copy-start = (f32[64,2048]{1,0:T(8,128)S(1)}, f32[64,2048]{1,0:T(8,128)}, u32[]{:S(2)}) copy-start(f32[64,2048]{1,0:T(8,128)} %get-tuple-element.7) | copy-start | bytes 1572868

commit v2 on v1

v2 whole, which is shorter than its diff:
```python
import functools

import jax
import jax.numpy as jnp
from jax import lax
from jax.experimental import pallas as pl
from jax.experimental.pallas import tpu as pltpu
from jax.sharding import PartitionSpec as P

HEADS = 32
KV_HEADS = 16
HEAD = 64
WINDOW = 128


EPS = 1e-06
NEGATIVE = -1e30
MESH = pl.DeviceIdType.MESH


def plane():
    t = lax.axis_index("tp")
    tx = t + 1 - 2 * lax.rem(t, 2)
    ty = lax.rem(t + 2, 4)
    return t, tx, ty, 3 - t


def remote(src, dst, send, recv, device):
    return pltpu.make_async_remote_copy(
        src_ref=src,
        dst_ref=dst,
        send_sem=send,
        recv_sem=recv,
        device_id=device,
        device_id_type=MESH,
    )


def flipped(index, mask):
    result = index
    bit = 1
    while bit <= mask:
        if mask & bit:
            result = result + bit * (1 - 2 * lax.rem(index // bit, 2))
        bit *= 2
    return result


def layer_kernel(
    q_hbm, k_hbm, v_hbm, sink_ref, w_hbm, res_hbm, gain_ref, routes_ref, route_weights_ref,
    gate_hbm, up_hbm, down_hbm, out_ref,
    q, kv, w, res, buf, acc, cols, got, state, gate, up, down,
    meta, meta_in, meta_z, meta_p, tok, xs, xo, hidden, po, ps, rt,
    bx1, by1, bx2, by2, mid, sz, zin, home_sum,
    load, hs, hr, gs, gr, as_, ar, ms, mr, zs, zr, ds_, dr, xs_s, xs_r, ps_s, ps_r,
    rs, rr, zbs, zbr,
):
    s = lax.axis_index("sp")
    t, tx, ty, td = plane()
    last = lax.axis_size("sp") - 1
    rows, depth = q.shape
    half = rows // 2
    groups = k_hbm.shape[1] // HEAD
    kept = groups * HEAD
    odd = lax.rem(s, 2)
    near = s + 1 - 2 * odd
    has_far = jnp.logical_and(s != 0, s != last)
    far = jnp.where(has_far, s - 1 + 2 * odd, near)
    x_dev, y_dev, d_dev, n_dev, f_dev = (s, tx), (s, ty), (s, td), (near, t), (far, t)
    z = s // 2
    planes = [flipped(z, m) for m in range(4)]
    z_devs = [(2 * planes[m] + odd, t) for m in range(4)]
    middle = pl.ds(half, rows)
    loads = [
        pltpu.make_async_copy(source, target, load.at[k])
        for k, (source, target) in enumerate(
            (
                (k_hbm, kv.at[middle, pl.ds(0, kept)]),
                (v_hbm, kv.at[middle, pl.ds(kept, kept)]),
                (q_hbm, q),
                (w_hbm, w),
                (res_hbm, res),
                (gate_hbm, gate),
                (up_hbm, up),
                (down_hbm, down),
            )
        )
    ]
    for copy in loads[:5]:
        copy.start()
    barrier = pltpu.get_barrier_semaphore()
    for device in [x_dev, y_dev, d_dev, n_dev] + z_devs[1:]:
        pl.semaphore_signal(barrier, inc=1, device_id=device, device_id_type=MESH)

    @pl.when(has_far)
    def _():
        pl.semaphore_signal(barrier, inc=1, device_id=f_dev, device_id_type=MESH)
        pl.semaphore_wait(barrier, 8)

    @pl.when(jnp.logical_not(has_far))
    def _():
        pl.semaphore_wait(barrier, 7)

    def aligned(value, size):
        return pl.ds(pl.multiple_of(value, size), size)

    near_src = aligned(2 * half - half * odd, half)
    near_dst = aligned(3 * half * odd, half)
    far_src = aligned(half + half * odd, half)
    far_dst = aligned(3 * half * (1 - odd), half)
    near_copy = remote(kv.at[near_src], kv.at[near_dst], hs.at[0], hr.at[0], n_dev)
    far_copy = remote(kv.at[far_src], kv.at[far_dst], hs.at[1], hr.at[1], f_dev)
    loads[0].wait()
    loads[1].wait()

    @pl.when(has_far)
    def _():
        far_copy.start()

    near_copy.start()
    copies = []

    def go(*args):
        copy = remote(*args)
        copy.start()
        copies.append(copy)
        return copy

    count, lanes = meta.shape[0] // 2, meta.shape[1]
    tokens = lanes // 4
    expert = lax.broadcasted_iota(jnp.int32, (count, lanes), 0)
    lane = lax.broadcasted_iota(jnp.int32, (count, lanes), 1)
    mine_lane = jnp.logical_and(lane >= t * tokens, lane < (t + 1) * tokens)
    hit_one = routes_ref[0:1, :] == expert
    hit = jnp.logical_and(mine_lane, jnp.logical_or(hit_one, routes_ref[1:2, :] == expert))
    chosen = jnp.where(hit, 1.0, 0.0)
    before = lax.broadcasted_iota(jnp.int32, (lanes, lanes), 0) <= lax.broadcasted_iota(
        jnp.int32, (lanes, lanes), 1
    )
    rank = jnp.dot(
        chosen.astype(jnp.bfloat16),
        jnp.where(before, 1.0, 0.0).astype(jnp.bfloat16),
        preferred_element_type=jnp.float32,
    )
    meta[0:count] = chosen * rank
    meta[count : 2 * count] = chosen * jnp.where(
        hit_one, route_weights_ref[0:1, :], route_weights_ref[1:2, :]
    )
    meta_copies = [
        go(meta, meta_in.at[t], ms.at[k], mr.at[k], device)
        for k, device in enumerate((x_dev, y_dev, d_dev))
    ]

    for copy in loads[5:]:
        copy.start()

    @pl.when(jnp.logical_not(has_far))
    def _():
        kv[aligned(3 * half * odd, half)] = jnp.zeros((half, kv.shape[1]), kv.dtype)

    loads[2].wait()
    span = 3 * half
    query = lax.broadcasted_iota(jnp.int32, (2 * half, span), 0)
    query = jnp.where(query >= half, query - half, query)
    key = lax.broadcasted_iota(jnp.int32, (2 * half, span), 1)
    band = jnp.abs(query + half - key) <= WINDOW
    upper = lax.broadcasted_iota(jnp.int32, (2 * half, 1), 0) < half

    def attend(b):
        valid = jnp.logical_and(
            band,
            jnp.logical_and(
                key >= jnp.where(2 * s + b == 0, half, 0),
                key < jnp.where(2 * s + b == 2 * last + 1, 2 * half, span),
            ),
        )
        keys_at = pl.ds(pl.multiple_of(b * half, half), span)
        mine = aligned(b * half, half)
        for g in range(groups):
            pair = q[mine, 2 * g * HEAD : 2 * (g + 1) * HEAD]
            stacked = jnp.concatenate([pair[:, :HEAD], pair[:, HEAD:]], axis=0)
            scores = lax.dot_general(
                stacked,
                kv[keys_at, g * HEAD : (g + 1) * HEAD],
                (((1,), (1,)), ((), ())),
                preferred_element_type=jnp.float32,
            ) * HEAD ** (-0.5)
            sink = jnp.where(upper, sink_ref[2 * g], sink_ref[2 * g + 1])
            masked = jnp.where(valid, scores, NEGATIVE)
            top = jnp.maximum(jnp.max(masked, axis=-1, keepdims=True), sink)
            probs = jnp.exp(masked - top)
            denom = jnp.sum(probs, axis=-1, keepdims=True) + jnp.exp(sink - top)
            weights = (probs * (1.0 / denom)).astype(jnp.bfloat16)
            output = jnp.dot(
                weights,
                kv[keys_at, kept + g * HEAD : kept + (g + 1) * HEAD],
                preferred_element_type=jnp.float32,
            )
            joined = jnp.concatenate([output[:half], output[half:]], axis=1)
            buf[t, mine, 2 * g * HEAD : 2 * (g + 1) * HEAD] = joined.astype(buf.dtype)

    first_block, second_block = 1 - odd, odd
    def spread(b, k):
        piece = buf.at[t, aligned(b * half, half)]
        return (
            go(piece, piece, gs.at[k], gr.at[k], x_dev),
            go(piece, piece, gs.at[k + 1], gr.at[k + 1], y_dev),
        )

    near_copy.wait_recv()
    attend(first_block)
    x_one, y_one = spread(first_block, 0)

    @pl.when(has_far)
    def _():
        far_copy.wait_recv()

    attend(second_block)
    x_two, y_two = spread(second_block, 2)
    for copy in meta_copies:
        copy.wait_recv()
    meta_z[z] = (meta[...] + meta_in[tx]) + (meta_in[ty] + meta_in[td])
    meta_z_copies = [
        go(meta_z.at[z], meta_z.at[z], ms.at[2 + m], mr.at[2 + m], z_devs[m]) for m in (1, 2, 3)
    ]
    loads[3].wait()

    def product(b, owner):
        weight = w[pl.ds(pl.multiple_of(owner * depth, depth), depth)]
        piece = buf[owner, aligned(b * half, half)]
        return jnp.dot(piece, weight, preferred_element_type=jnp.float32)

    x_one.wait_recv()
    piece = buf.at[tx, aligned(first_block * half, half)]
    d_one = go(piece, piece, gs.at[4], gr.at[4], y_dev)
    acc[0] = product(first_block, t)
    acc[0] += product(first_block, tx)
    y_one.wait_recv()
    acc[0] += product(first_block, ty)
    y_two.wait_recv()
    piece = buf.at[ty, aligned(second_block * half, half)]
    d_two = go(piece, piece, gs.at[5], gr.at[5], x_dev)
    acc[1] = product(second_block, t)
    acc[1] += product(second_block, ty)
    own = rows // 4
    to_x = remote(
        cols.at[aligned(tx * own, own)], got.at[t], as_.at[0], ar.at[0], x_dev
    )
    to_y = remote(
        cols.at[aligned(ty * own, own)], got.at[t], as_.at[1], ar.at[1], y_dev
    )
    to_d = remote(
        cols.at[aligned(td * own, own)], got.at[t], as_.at[2], ar.at[2], d_dev
    )
    home = t // 2

    def finish(b, k):
        total = acc[k] + product(b, td)
        cols[aligned(b * half, half)] = total.astype(cols.dtype)

        @pl.when(home == b)
        def _():
            to_x.start()

        @pl.when(home != b)
        def _():
            to_d.start()
            to_y.start()

    d_one.wait_recv()
    finish(first_block, 0)
    x_two.wait_recv()
    acc[1] += product(second_block, tx)
    d_two.wait_recv()
    finish(second_block, 1)
    got[t] = cols[aligned(t * own, own)]
    loads[4].wait()
    to_x.wait_recv()
    to_y.wait_recv()
    to_d.wait_recv()
    squares = jnp.zeros((own, 1), jnp.float32)
    width = w.shape[1]
    for k in range(4):
        columns = slice(k * width, (k + 1) * width)
        value = res[:, columns].astype(jnp.float32) + got[k].astype(jnp.float32)
        state[:, columns] = value
        squares += jnp.sum(value * value, axis=-1, keepdims=True)
    inverse = lax.rsqrt(squares * (1.0 / (4 * width)) + EPS)
    for k in range(4):
        columns = slice(k * width, (k + 1) * width)
        tok[t, z, :, columns] = (state[:, columns] * inverse * gain_ref[:, columns]).astype(
            tok.dtype
        )
    low, high = pl.ds(0, own // 2), pl.ds(own // 2, own // 2)
    z_copies = {
        m: go(tok.at[t, z], tok.at[t, z], zs.at[m], zr.at[m], z_devs[m]) for m in (1, 3, 2)
    }
    sent, forwarded, picks, parts, firsts, seconds, homes = {}, {}, {}, {}, {}, {}, {}

    def send(m):
        if m:
            z_copies[m].wait_recv()
        lower, upper = tok.at[t, planes[m], low], tok.at[t, planes[m], high]
        sent[m] = (
            go(lower, lower, ds_.at[m, 0], dr.at[m, 0], x_dev),
            go(upper, upper, ds_.at[m, 1], dr.at[m, 1], y_dev),
            go(upper, upper, ds_.at[m, 2], dr.at[m, 2], x_dev),
            go(lower, lower, ds_.at[m, 3], dr.at[m, 3], y_dev),
        )

    def forward(m):
        sent[m][0].wait_recv()
        block = tok.at[tx, planes[m], low]
        to_side = go(block, block, ds_.at[m, 4], dr.at[m, 4], y_dev)
        sent[m][1].wait_recv()
        block = tok.at[ty, planes[m], high]
        forwarded[m] = (to_side, go(block, block, ds_.at[m, 5], dr.at[m, 5], x_dev))

    slots = xo.shape[1]
    capacity = slots // 4
    step = 256
    model = tok.shape[3]
    row = lax.broadcasted_iota(jnp.int32, (slots, lanes), 0).astype(jnp.float32)
    shift = (lax.broadcasted_iota(jnp.int32, (1, lanes), 1) // tokens * capacity).astype(
        jnp.float32
    )
    mine_expert, near_expert = s, near

    def place(source, m, which):
        ranks = source[planes[m], pl.ds(which, 1), :]
        target = jnp.where(ranks > 0.5, ranks + (shift - 1.0), -1.0)
        return row == target

    def scale(source, m, which):
        weights = source[planes[m], pl.ds(count + which, 1), :]
        return jnp.sum(
            jnp.where(place(source, m, which), weights, 0.0), axis=1, keepdims=True
        )

    def picking(m):
        return jnp.concatenate(
            [
                jnp.where(place(meta_z, m, which), 1.0, 0.0)
                for which in (mine_expert, near_expert)
            ],
            axis=0,
        )

    def pick(m):
        for copy in sent[m][2:] + forwarded[m]:
            copy.wait_recv()
        chooser = picking(m).astype(jnp.bfloat16)
        for k in range(model // step):
            columns = slice(k * step, (k + 1) * step)
            rows_in = tok[:, planes[m], :, columns].reshape(lanes, step)
            found = jnp.dot(chooser, rows_in, preferred_element_type=jnp.float32)
            found = found.astype(xs.dtype)
            xs[m, 0:slots, columns] = found[:slots]
            xo[m, :, columns] = found[slots:]
        picks[m] = go(
            xo.at[m], xs.at[m, pl.ds(slots, slots)], xs_s.at[m], xs_r.at[m], n_dev
        )

    def rise(m, begin, end):
        @pl.loop(begin, end)
        def _(k):
            columns = pl.ds(pl.multiple_of(k * step, step), step)
            x = xs[m]
            g = jnp.dot(x, gate[:, columns], preferred_element_type=jnp.float32)
            u = jnp.dot(x, up[:, columns], preferred_element_type=jnp.float32)
            hidden[:, columns] = (jax.nn.silu(g) * u).astype(hidden.dtype)

    total_steps = gate.shape[1] // step
    first_steps = (total_steps + 1) // 2

    def fall(m):
        factor_mine = scale(meta_z, m, mine_expert)
        factor_near = scale(meta_p, m, mine_expert)
        wide = 512

        @pl.loop(0, model // wide)
        def _(k):
            columns = pl.ds(pl.multiple_of(k * wide, wide), wide)
            share = jnp.dot(hidden[...], down[:, columns], preferred_element_type=jnp.float32)
            po[m, 0:slots, columns] = (share[:slots] * factor_mine).astype(po.dtype)
            ps[m, :, columns] = (share[slots:] * factor_near).astype(ps.dtype)

        parts[m] = go(
            ps.at[m], po.at[m, pl.ds(slots, slots)], ps_s.at[m], ps_r.at[m], n_dev
        )

    def expand(m):
        parts[m].wait_recv()
        spreader = picking(m).T.astype(jnp.bfloat16)
        for k in range(model // step):
            columns = slice(k * step, (k + 1) * step)
            found = jnp.dot(spreader, po[m, :, columns], preferred_element_type=jnp.float32)
            rt[m, :, :, columns] = found.astype(rt.dtype).reshape(4, tokens, step)

    def reduce_one(m):
        firsts[m] = (
            go(rt.at[m, td, low], bx1.at[m, 1], rs.at[m, 0], rr.at[m, 0], x_dev),
            go(rt.at[m, td, high], by1.at[m, 1], rs.at[m, 1], rr.at[m, 1], y_dev),
            go(rt.at[m, tx, low], bx1.at[m, 0], rs.at[m, 2], rr.at[m, 2], x_dev),
            go(rt.at[m, ty, high], by1.at[m, 0], rs.at[m, 3], rr.at[m, 3], y_dev),
        )

    def wide_sum(*pieces):
        result = pieces[0].astype(jnp.float32)
        for piece in pieces[1:]:
            result = result + piece.astype(jnp.float32)
        return result

    def reduce_two(m):
        firsts[m][0].wait_recv()
        mid[m, 0] = wide_sum(rt[m, ty, low], bx1[m, 1]).astype(mid.dtype)
        to_side = go(mid.at[m, 0], by2.at[m], rs.at[m, 4], rr.at[m, 4], y_dev)
        firsts[m][1].wait_recv()
        mid[m, 1] = wide_sum(rt[m, tx, high], by1[m, 1]).astype(mid.dtype)
        seconds[m] = (
            to_side,
            go(mid.at[m, 1], bx2.at[m], rs.at[m, 5], rr.at[m, 5], x_dev),
        )

    def reduce_three(m):
        firsts[m][2].wait_recv()
        seconds[m][0].wait_recv()
        lower = wide_sum(rt[m, t, low], bx1[m, 0], by2[m])
        firsts[m][3].wait_recv()
        seconds[m][1].wait_recv()
        upper = wide_sum(rt[m, t, high], by1[m, 0], bx2[m])
        if m:
            sz[m, low] = lower.astype(sz.dtype)
            sz[m, high] = upper.astype(sz.dtype)
            homes[m] = go(sz.at[m], zin.at[m], zbs.at[m], zbr.at[m], z_devs[m])
        else:
            home_sum[low] = lower
            home_sum[high] = upper

    send(0)
    forward(0)
    for copy in meta_z_copies:
        copy.wait_recv()
    meta_near = go(meta_z, meta_p, ms.at[6], mr.at[6], n_dev)
    send(1)
    pick(0)
    for copy in loads[5:]:
        copy.wait()
    picks[0].wait_recv()
    rise(0, 0, first_steps)
    forward(1)
    send(3)
    rise(0, first_steps, total_steps)
    meta_near.wait_recv()
    fall(0)
    pick(1)
    picks[1].wait_recv()
    rise(1, 0, first_steps)
    forward(3)
    send(2)
    rise(1, first_steps, total_steps)
    fall(1)
    pick(3)
    picks[3].wait_recv()
    rise(3, 0, first_steps)
    forward(2)
    rise(3, first_steps, total_steps)
    fall(3)
    expand(3)
    reduce_one(3)
    pick(2)
    picks[2].wait_recv()
    rise(2, 0, first_steps)
    reduce_two(3)
    rise(2, first_steps, total_steps)
    fall(2)
    expand(2)
    reduce_one(2)
    reduce_three(3)
    expand(1)
    reduce_one(1)
    reduce_two(2)
    expand(0)
    reduce_one(0)
    reduce_three(2)
    reduce_two(1)
    reduce_three(1)
    reduce_two(0)
    reduce_three(0)
    for m in (3, 2, 1):
        homes[m].wait_recv()
    out_ref[...] = (
        state[...] + (home_sum[...] + wide_sum(zin[1], zin[2], zin[3]))
    ).astype(out_ref.dtype)
    for copy in copies:
        copy.wait_send()
    near_copy.wait_send()
    to_x.wait_send()
    to_y.wait_send()
    to_d.wait_send()

    @pl.when(has_far)
    def _():
        far_copy.wait_send()


def layer(
    queries, keys, values, sink_logit, out_weight, residual, norm_gain, routes, route_weights,
    gate_weight, up_weight, down_weight, capacity,
):
    rows, depth = queries.shape
    kind = queries.dtype
    width = out_weight.shape[1]
    tokens, model = residual.shape
    count = lax.axis_size("sp")
    slots = 4 * capacity
    anywhere = pl.BlockSpec(memory_space=pl.ANY)
    vmem = pl.BlockSpec(memory_space=pltpu.VMEM)
    dma = pltpu.SemaphoreType.DMA
    one, six = dma((4,)), dma((4, 6))
    lanes = 4 * tokens
    return pl.pallas_call(
        layer_kernel,
        out_shape=jax.ShapeDtypeStruct(residual.shape, kind),
        in_specs=[anywhere] * 3
        + [pl.BlockSpec(memory_space=pltpu.SMEM), anywhere, anywhere, vmem, vmem, vmem]
        + [anywhere] * 3,
        out_specs=vmem,
        scratch_shapes=[
            pltpu.VMEM(queries.shape, kind),
            pltpu.VMEM((2 * rows, 2 * keys.shape[1]), kind),
            pltpu.VMEM(out_weight.shape, kind),
            pltpu.VMEM(residual.shape, kind),
            pltpu.VMEM((4, rows, depth), kind),
            pltpu.VMEM((2, rows // 2, width), jnp.float32),
            pltpu.VMEM((rows, width), kind),
            pltpu.VMEM((4, rows // 4, width), kind),
            pltpu.VMEM(residual.shape, jnp.float32),
            pltpu.VMEM(gate_weight.shape, kind),
            pltpu.VMEM(up_weight.shape, kind),
            pltpu.VMEM(down_weight.shape, kind),
            pltpu.VMEM((2 * count, lanes), jnp.float32),
            pltpu.VMEM((4, 2 * count, lanes), jnp.float32),
            pltpu.VMEM((4, 2 * count, lanes), jnp.float32),
            pltpu.VMEM((4, 2 * count, lanes), jnp.float32),
            pltpu.VMEM((4, 4, tokens, model), kind),
            pltpu.VMEM((4, 2 * slots, model), kind),
            pltpu.VMEM((4, slots, model), kind),
            pltpu.VMEM((2 * slots, gate_weight.shape[1]), kind),
            pltpu.VMEM((4, 2 * slots, model), kind),
            pltpu.VMEM((4, slots, model), kind),
            pltpu.VMEM((4, 4, tokens, model), kind),
            pltpu.VMEM((4, 2, tokens // 2, model), kind),
            pltpu.VMEM((4, 2, tokens // 2, model), kind),
            pltpu.VMEM((4, tokens // 2, model), kind),
            pltpu.VMEM((4, tokens // 2, model), kind),
            pltpu.VMEM((4, 2, tokens // 2, model), kind),
            pltpu.VMEM((4, tokens, model), kind),
            pltpu.VMEM((4, tokens, model), kind),
            pltpu.VMEM(residual.shape, jnp.float32),
            dma((8,)),
            dma((2,)),
            dma((2,)),
            dma((6,)),
            dma((6,)),
            dma((3,)),
            dma((3,)),
            dma((7,)),
            dma((7,)),
            one, one, six, six, one, one, one, one, six, six, one, one,
        ],
        compiler_params=pltpu.CompilerParams(
            collective_id=0, has_side_effects=True, vmem_limit_bytes=60 * 1024 * 1024
        ),
    )(
        queries, keys, values, sink_logit, out_weight, residual, norm_gain.reshape(1, -1),
        jnp.tile(routes.T, (1, 4)), jnp.tile(route_weights.T, (1, 4)),
        gate_weight, up_weight, down_weight,
    )


def with_halo(block, sides, width):
    for axis, dim in sides:
        count = lax.axis_size(axis)
        forward = [(i, i + 1) for i in range(count - 1)]
        backward = [(target, source) for source, target in forward]
        low = lax.ppermute(
            lax.slice_in_dim(block, block.shape[dim] - width, None, axis=dim), axis, forward
        )
        high = lax.ppermute(lax.slice_in_dim(block, 0, width, axis=dim), axis, backward)
        block = jnp.concatenate([low, block, high], axis=dim)
    return block


def make_band(extended, length):
    blocks = length // WINDOW
    pieces = [
        lax.slice_in_dim(extended, offset * WINDOW, offset * WINDOW + length, axis=0).reshape(
            blocks, WINDOW, -1
        )
        for offset in range(3)
    ]
    return jnp.concatenate(pieces, axis=1)


def attend_local(queries, keys, values, sink_logit):
    length = queries.shape[0]
    groups = keys.shape[1] // HEAD
    repeat = HEADS // KV_HEADS
    blocks = length // WINDOW
    joined = jnp.concatenate([keys, values], axis=1)
    extended = with_halo(joined, (("sp", 0),), WINDOW)
    banded = make_band(extended, length)
    key_band = banded[..., : groups * HEAD].reshape(blocks, 3 * WINDOW, groups, HEAD)
    value_band = banded[..., groups * HEAD :].reshape(blocks, 3 * WINDOW, groups, HEAD)
    query_blocks = queries.reshape(blocks, WINDOW, groups, repeat, HEAD)
    scores = jnp.einsum(
        "nqgrd,nkgd->ngrqk", query_blocks, key_band, preferred_element_type=jnp.float32
    ) * HEAD ** (-0.5)
    near = jnp.abs(jnp.arange(WINDOW)[:, None] + WINDOW - jnp.arange(3 * WINDOW)[None, :]) <= WINDOW
    first_token = lax.axis_index("sp") * length
    key_pos = (
        first_token + (jnp.arange(blocks)[:, None] - 1) * WINDOW + jnp.arange(3 * WINDOW)[None, :]
    )
    inside = (key_pos >= 0) & (key_pos < length * lax.axis_size("sp"))
    valid = near[None, None, None, :, :] & inside[:, None, None, None, :]
    sinks = sink_logit.reshape(1, groups, repeat, 1, 1)
    masked = jnp.where(valid, scores, NEGATIVE)
    top = jnp.maximum(jnp.max(masked, axis=-1, keepdims=True), sinks)
    probs = jnp.exp(masked - top)
    denom = jnp.sum(probs, axis=-1, keepdims=True) + jnp.exp(sinks - top)
    weights = (probs / denom).astype(jnp.bfloat16)
    output = jnp.einsum(
        "ngrqk,nkgd->nqgrd", weights, value_band, preferred_element_type=jnp.float32
    )
    return output.astype(jnp.bfloat16).reshape(length, groups * repeat * HEAD)


def local(
    queries,
    keys,
    values,
    sink_logit,
    out_weight,
    residual,
    norm_gain,
    routes,
    route_weights,
    gate_weight,
    up_weight,
    down_weight,
):
    capacity = max(2, 4 * residual.shape[0] // lax.axis_size("sp"))
    in_plane = (
        lax.axis_size("tp") == 4
        and lax.axis_size("sp") == 8
        and capacity % 32 == 0
        and gate_weight.shape[2] % 256 == 0
        and queries.shape[0] == 2 * WINDOW
        and residual.shape[0] == 64
    )
    if in_plane:
        return layer(
            queries, keys, values, sink_logit, out_weight, residual, norm_gain, routes,
            route_weights, gate_weight[0], up_weight[0], down_weight[0], capacity,
        )
    attention = attend_local(queries, keys, values, sink_logit)
    columns = jnp.dot(
        lax.all_gather(attention, "tp", axis=1, tiled=True),
        out_weight,
        preferred_element_type=jnp.float32,
    )
    projected = lax.all_to_all(
        columns.astype(jnp.bfloat16), "tp", split_axis=0, concat_axis=1, tiled=True
    )
    hidden_state = residual.astype(jnp.float32) + projected.astype(jnp.float32)
    inverse = lax.rsqrt(jnp.mean(hidden_state * hidden_state, axis=-1, keepdims=True) + EPS)
    normed = (hidden_state * inverse * norm_gain).astype(jnp.bfloat16)
    sp_count = lax.axis_size("sp")
    tok_rows = residual.shape[0]
    width = residual.shape[1]
    slot_total = sp_count * capacity
    expert_ids = routes.reshape(-1)
    onehot = (expert_ids[:, None] == jnp.arange(sp_count, dtype=jnp.int32)[None, :]).astype(
        jnp.int32
    )
    earlier = jnp.cumsum(onehot, axis=0) - onehot
    rank = jnp.sum(earlier * onehot, axis=1)
    slots = expert_ids * capacity + rank
    placing = (slots[:, None] == jnp.arange(slot_total, dtype=jnp.int32)[None, :]).astype(
        jnp.bfloat16
    )
    placing = placing.reshape(tok_rows, 2, slot_total)
    first_place = placing[:, 0]
    second_place = placing[:, 1]
    sending = jnp.einsum(
        "ts,td->sd", first_place + second_place, normed, preferred_element_type=jnp.float32
    )
    sending = sending.astype(jnp.bfloat16).reshape(sp_count, capacity, width)
    piece = lax.all_gather(
        lax.all_to_all(sending, "sp", split_axis=0, concat_axis=0, tiled=True),
        "tp",
        axis=0,
        tiled=True,
    )
    flat = piece.reshape(-1, piece.shape[-1])
    gate = jnp.dot(flat, gate_weight[0], preferred_element_type=jnp.float32)
    upward = jnp.dot(flat, up_weight[0], preferred_element_type=jnp.float32)
    hidden = (jax.nn.silu(gate) * upward).astype(jnp.bfloat16)
    partial_value = jnp.dot(hidden, down_weight[0], preferred_element_type=jnp.float32)
    partial_value = partial_value.reshape(piece.shape[:-1] + (down_weight.shape[-1],))
    returned = lax.all_to_all(
        lax.psum_scatter(
            partial_value.astype(jnp.bfloat16), "tp", scatter_dimension=0, tiled=True
        ),
        "sp",
        split_axis=0,
        concat_axis=0,
        tiled=True,
    )
    gathered_back = returned.reshape(slot_total, width)
    first_pick = jnp.dot(first_place, gathered_back, preferred_element_type=jnp.float32)
    second_pick = jnp.dot(second_place, gathered_back, preferred_element_type=jnp.float32)
    mixture = route_weights[:, 0:1] * first_pick + route_weights[:, 1:2] * second_pick
    return (hidden_state + mixture).astype(jnp.bfloat16)


def solution(mesh):
    in_specs = (
        P("sp", "tp"),
        P("sp", "tp"),
        P("sp", "tp"),
        P("tp"),
        P(None, "tp"),
        P(("sp", "tp"), None),
        P(),
        P(("sp", "tp"), None),
        P(("sp", "tp"), None),
        P("sp", None, "tp"),
        P("sp", None, "tp"),
        P("sp", "tp", None),
    )
    out_specs = P(("sp", "tp"), None)
    return jax.shard_map(local, mesh=mesh, in_specs=in_specs, out_specs=out_specs, check_vma=False)
```

time: 123 us -> 119 us (0.967)
  matrix products: 6.16 us -> 0 us
  local copies, waits for them, and re-layouts: 1.13 us -> 4.34 us
    dot_general x3 -> x0, matrix products: 6.16 us -> none  [the longest x1 2.4 us: local(): jnp.einsum('ts,td->sd', first_place + second_place, normed, preferred_ele...]
    another operation x0 -> x4, local copies, waits for them, and re-layouts: none -> 2.67 us  [the longest x2 1.34 us: layer(): jnp.tile(routes.T, (1, 4))]
    pallas_call x2 -> x1, Pallas kernels: 114 us -> 115 us  [layer(): pl.pallas_call(layer_kernel, out_shape=jax.ShapeDtypeStruct(residual.shap...]
where the time goes in v2:
time: 119 us
  Pallas kernels  115 us (97%)
  local copies, waits for them, and re-layouts  4.34 us (4%)
    pallas_call x1, Pallas kernels, layer(): pl.pallas_call(layer_kernel, out_shape=jax.ShapeDtypeStruct(residual.shap...  115 us

profile of v2, /device:TPU:0, one launch (start us, length us, event | category | flops | bytes accessed | tf_op | source)
XLA Modules:
  0.0 119.2 jit_solution(12039107754531208347)
XLA Ops:
  0.0 0.7 tile.8
  0.7 0.7 tile.9.routes_ref
  1.3 0.7 tile.20
  2.0 0.7 tile.21.route_weights_ref
  2.7 114.9 %shard_map.118 = bf16[64,2048]{1,0:T(8,128)(2,1)} custom-call(bf16[256,512]{1,0:T(8,128)(2,1)} %q_hbm.1, bf16[256,256]{1,0:T(8,128)(2,1)} %k_hbm.1, bf16[256,256]{1,0:T(8,128)(2,1)} %v_hbm.1, f32[8]{0:T(128)} %sink_ref.1, bf16[2048,512]{1,0:T(8,128)(2,1)} %w_hbm.1, bf16[64,2048]{1,0:T(8,128)(2,1)} %res_hbm.1, f32[1,2048]{1,0:T(1,128)} %bitcast.9, ...), custom_call_target="tpu_custom_call" | custom-call | tf_op jit(solution)/shard_map/pallas_call | solution.py:522
  117.6 1.7 %copy.14 = bf16[64,2048]{1,0:T(8,128)(2,1)} copy(bf16[64,2048]{1,0:T(8,128)(2,1)} %shard_map.118) | data formatting | bytes 524288

commit v3 on v2

--- a/solution.py
+++ b/solution.py
@@ -49,10 +49,10 @@
 def layer_kernel(
     q_hbm, k_hbm, v_hbm, sink_ref, w_hbm, res_hbm, gain_ref, routes_ref, route_weights_ref,
     gate_hbm, up_hbm, down_hbm, out_ref,
-    q, kv, w, res, buf, acc, cols, got, state, gate, up, down,
-    meta, meta_in, meta_z, meta_p, tok, xs, xo, hidden, po, ps, rt,
+    q, kv, w, res, res_in, buf, acc, proj, gate, up, down,
+    meta, meta_in, meta_z, meta_p, squares, squares_in, inverse, tok, xs, xo, hidden, po, ps, rt,
     bx1, by1, bx2, by2, mid, sz, zin, home_sum,
-    load, hs, hr, gs, gr, as_, ar, ms, mr, zs, zr, ds_, dr, xs_s, xs_r, ps_s, ps_r,
+    load, hs, hr, gs, gr, as_, ar, ms, mr, qs, qr, zs, zr, ds_, dr, xs_s, xs_r, ps_s, ps_r,
     rs, rr, zbs, zbr,
 ):
     s = lax.axis_index("sp")
@@ -70,6 +70,8 @@
     z = s // 2
     planes = [flipped(z, m) for m in range(4)]
     z_devs = [(2 * planes[m] + odd, t) for m in range(4)]
+    inner = jnp.logical_or(z == 1, z == 2)
+    outer = jnp.logical_not(inner)
     middle = pl.ds(half, rows)
     loads = [
         pltpu.make_async_copy(source, target, load.at[k])
@@ -126,13 +128,29 @@
         copies.append(copy)
         return copy
 
+    own, model = res.shape
+    width = w.shape[1]
+    loads[4].wait()
+    res_copies = [
+        go(
+            res.at[:, aligned(owner * width, width)],
+            res_in.at[t],
+            as_.at[k],
+            ar.at[k],
+            device,
+        )
+        for k, (owner, device) in enumerate(((tx, x_dev), (ty, y_dev), (td, d_dev)))
+    ]
+    res_in[t] = res[:, aligned(t * width, width)]
     count, lanes = meta.shape[0] // 2, meta.shape[1]
     tokens = lanes // 4
     expert = lax.broadcasted_iota(jnp.int32, (count, lanes), 0)
     lane = lax.broadcasted_iota(jnp.int32, (count, lanes), 1)
     mine_lane = jnp.logical_and(lane >= t * tokens, lane < (t + 1) * tokens)
-    hit_one = routes_ref[0:1, :] == expert
-    hit = jnp.logical_and(mine_lane, jnp.logical_or(hit_one, routes_ref[1:2, :] == expert))
+    routes = jnp.concatenate([routes_ref[...]] * 4, axis=1)
+    route_weights = jnp.concatenate([route_weights_ref[...]] * 4, axis=1)
+    hit_one = routes[0:1, :] == expert
+    hit = jnp.logical_and(mine_lane, jnp.logical_or(hit_one, routes[1:2, :] == expert))
     chosen = jnp.where(hit, 1.0, 0.0)
     before = lax.broadcasted_iota(jnp.int32, (lanes, lanes), 0) <= lax.broadcasted_iota(
         jnp.int32, (lanes, lanes), 1
@@ -144,7 +162,7 @@
     )
     meta[0:count] = chosen * rank
     meta[count : 2 * count] = chosen * jnp.where(
-        hit_one, route_weights_ref[0:1, :], route_weights_ref[1:2, :]
+        hit_one, route_weights[0:1, :], route_weights[1:2, :]
     )
     meta_copies = [
         go(meta, meta_in.at[t], ms.at[k], mr.at[k], device)
@@ -199,24 +217,26 @@
             joined = jnp.concatenate([output[:half], output[half:]], axis=1)
             buf[t, mine, 2 * g * HEAD : 2 * (g + 1) * HEAD] = joined.astype(buf.dtype)
 
-    first_block, second_block = 1 - odd, odd
-    def spread(b, k):
-        piece = buf.at[t, aligned(b * half, half)]
+    blocks = (1 - odd, odd)
+    parts_of = [aligned(b * half, half) for b in blocks]
+
+    def spread(h, k):
+        piece = buf.at[t, parts_of[h]]
         return (
             go(piece, piece, gs.at[k], gr.at[k], x_dev),
             go(piece, piece, gs.at[k + 1], gr.at[k + 1], y_dev),
         )
 
     near_copy.wait_recv()
-    attend(first_block)
-    x_one, y_one = spread(first_block, 0)
+    attend(blocks[0])
+    x_one, y_one = spread(0, 0)
 
     @pl.when(has_far)
     def _():
         far_copy.wait_recv()
 
-    attend(second_block)
-    x_two, y_two = spread(second_block, 2)
+    attend(blocks[1])
+    x_two, y_two = spread(1, 2)
     for copy in meta_copies:
         copy.wait_recv()
     meta_z[z] = (meta[...] + meta_in[tx]) + (meta_in[ty] + meta_in[td])
@@ -224,107 +244,101 @@
         go(meta_z.at[z], meta_z.at[z], ms.at[2 + m], mr.at[2 + m], z_devs[m]) for m in (1, 2, 3)
     ]
     loads[3].wait()
-
-    def product(b, owner):
+    for copy in res_copies:
+        copy.wait_recv()
+
+    def product(h, owner):
         weight = w[pl.ds(pl.multiple_of(owner * depth, depth), depth)]
-        piece = buf[owner, aligned(b * half, half)]
-        return jnp.dot(piece, weight, preferred_element_type=jnp.float32)
+        return jnp.dot(buf[owner, parts_of[h]], weight, preferred_element_type=jnp.float32)
 
     x_one.wait_recv()
-    piece = buf.at[tx, aligned(first_block * half, half)]
+    piece = buf.at[tx, parts_of[0]]
     d_one = go(piece, piece, gs.at[4], gr.at[4], y_dev)
-    acc[0] = product(first_block, t)
-    acc[0] += product(first_block, tx)
+    acc[0] = product(0, t)
+    acc[0] += product(0, tx)
     y_one.wait_recv()
-    acc[0] += product(first_block, ty)
+    acc[0] += product(0, ty)
     y_two.wait_recv()
-    piece = buf.at[ty, aligned(second_block * half, half)]
+    piece = buf.at[ty, parts_of[1]]
     d_two = go(piece, piece, gs.at[5], gr.at[5], x_dev)
-    acc[1] = product(second_block, t)
-    acc[1] += product(second_block, ty)
-    own = rows // 4
-    to_x = remote(
-        cols.at[aligned(tx * own, own)], got.at[t], as_.at[0], ar.at[0], x_dev
-    )
-    to_y = remote(
-        cols.at[aligned(ty * own, own)], got.at[t], as_.at[1], ar.at[1], y_dev
-    )
-    to_d = remote(
-        cols.at[aligned(td * own, own)], got.at[t], as_.at[2], ar.at[2], d_dev
-    )
-    home = t // 2
-
-    def finish(b, k):
-        total = acc[k] + product(b, td)
-        cols[aligned(b * half, half)] = total.astype(cols.dtype)
-
-        @pl.when(home == b)
+    acc[1] = product(1, t)
+    acc[1] += product(1, ty)
+    gain = gain_ref[:, aligned(t * width, width)]
+
+    def finish(h):
+        projected = (acc[h] + product(h, td)).astype(proj.dtype)
+        proj[parts_of[h]] = projected
+        pair = res_in[pl.ds(2 * blocks[h], 2)].reshape(half, width)
+        value = pair.astype(jnp.float32) + projected.astype(jnp.float32)
+        tok[t, z, parts_of[h]] = (value * gain).astype(tok.dtype)
+        return jnp.sum(value * value, axis=-1, keepdims=True)
+
+    def record(h, sums):
+        squares[blocks[h]] = jnp.broadcast_to(sums, (half, half)).T[: squares.shape[1]]
+
+    def own_block(h):
+        return tok.at[t, z, parts_of[h]]
+
+    z_in = {
+        (m, h): remote(
+            own_block(h), tok.at[t, planes[m], parts_of[h]], zs.at[m, h], zr.at[m, h], z_devs[m]
+        )
+        for m in (1, 2, 3)
+        for h in (0, 1)
+    }
+
+    out_one = [remote(own_block(h), own_block(h), zs.at[1, h], zr.at[1, h], z_devs[1]) for h in (0, 1)]
+    out_three = [remote(own_block(h), own_block(h), zs.at[3, h], zr.at[3, h], z_devs[3]) for h in (0, 1)]
+
+    def relay_copy(m, h):
+        piece = tok.at[t, planes[m], parts_of[h]]
+        lands, device = ((2, z_devs[3]), None, (3, z_devs[1]), (2, z_devs[1]))[
+            {1: 0, 2: 2, 3: 3}[m]
+        ]
+        return remote(piece, piece, zs.at[3 + m, h], zr.at[lands, h], device)
+
+    def depart(h):
+        out_one[h].start()
+
+        @pl.when(inner)
         def _():
-            to_x.start()
-
-        @pl.when(home != b)
+            out_three[h].start()
+
+    sent, forwarded, picks, parts, firsts, seconds, homes = {}, {}, {}, {}, {}, {}, {}
+
+    def arrive(m, h):
+        z_in[m, h].wait_recv()
+
+    def relay(m, h, waited=True):
+        @pl.when(inner)
         def _():
-            to_d.start()
-            to_y.start()
-
-    d_one.wait_recv()
-    finish(first_block, 0)
-    x_two.wait_recv()
-    acc[1] += product(second_block, tx)
-    d_two.wait_recv()
-    finish(second_block, 1)
-    got[t] = cols[aligned(t * own, own)]
-    loads[4].wait()
-    to_x.wait_recv()
-    to_y.wait_recv()
-    to_d.wait_recv()
-    squares = jnp.zeros((own, 1), jnp.float32)
-    width = w.shape[1]
-    for k in range(4):
-        columns = slice(k * width, (k + 1) * width)
-        value = res[:, columns].astype(jnp.float32) + got[k].astype(jnp.float32)
-        state[:, columns] = value
-        squares += jnp.sum(value * value, axis=-1, keepdims=True)
-    inverse = lax.rsqrt(squares * (1.0 / (4 * width)) + EPS)
-    for k in range(4):
-        columns = slice(k * width, (k + 1) * width)
-        tok[t, z, :, columns] = (state[:, columns] * inverse * gain_ref[:, columns]).astype(
-            tok.dtype
-        )
-    low, high = pl.ds(0, own // 2), pl.ds(own // 2, own // 2)
-    z_copies = {
-        m: go(tok.at[t, z], tok.at[t, z], zs.at[m], zr.at[m], z_devs[m]) for m in (1, 3, 2)
-    }
-    sent, forwarded, picks, parts, firsts, seconds, homes = {}, {}, {}, {}, {}, {}, {}
-
-    def send(m):
-        if m:
-            z_copies[m].wait_recv()
-        lower, upper = tok.at[t, planes[m], low], tok.at[t, planes[m], high]
-        sent[m] = (
-            go(lower, lower, ds_.at[m, 0], dr.at[m, 0], x_dev),
-            go(upper, upper, ds_.at[m, 1], dr.at[m, 1], y_dev),
-            go(upper, upper, ds_.at[m, 2], dr.at[m, 2], x_dev),
-            go(lower, lower, ds_.at[m, 3], dr.at[m, 3], y_dev),
-        )
-
-    def forward(m):
-        sent[m][0].wait_recv()
-        block = tok.at[tx, planes[m], low]
-        to_side = go(block, block, ds_.at[m, 4], dr.at[m, 4], y_dev)
-        sent[m][1].wait_recv()
-        block = tok.at[ty, planes[m], high]
-        forwarded[m] = (to_side, go(block, block, ds_.at[m, 5], dr.at[m, 5], x_dev))
+            if not waited:
+                arrive(m, h)
+            relay_copy(m, h).start()
+
+    def send(m, h):
+        piece = tok.at[t, planes[m], parts_of[h]]
+        sent[m, h] = (
+            go(piece, piece, ds_.at[m, 2 * h], dr.at[m, 2 * h], x_dev),
+            go(piece, piece, ds_.at[m, 2 * h + 1], dr.at[m, 2 * h + 1], y_dev),
+        )
+
+    def forward(m, h):
+        sent[m, h][0].wait_recv()
+        piece = tok.at[tx, planes[m], aligned(blocks[h] * half, half // 2)]
+        first = go(piece, piece, ds_.at[m, 4 + 2 * h], dr.at[m, 4 + 2 * h], y_dev)
+        sent[m, h][1].wait_recv()
+        piece = tok.at[ty, planes[m], aligned(blocks[h] * half + half // 2, half // 2)]
+        second = go(piece, piece, ds_.at[m, 5 + 2 * h], dr.at[m, 5 + 2 * h], x_dev)
+        forwarded[m, h] = (first, second)
 
     slots = xo.shape[1]
     capacity = slots // 4
     step = 256
-    model = tok.shape[3]
     row = lax.broadcasted_iota(jnp.int32, (slots, lanes), 0).astype(jnp.float32)
     shift = (lax.broadcasted_iota(jnp.int32, (1, lanes), 1) // tokens * capacity).astype(
         jnp.float32
     )
-    mine_expert, near_expert = s, near
 
     def place(source, m, which):
         ranks = source[planes[m], pl.ds(which, 1), :]
@@ -339,24 +353,28 @@
 
     def picking(m):
         return jnp.concatenate(
-            [
-                jnp.where(place(meta_z, m, which), 1.0, 0.0)
-                for which in (mine_expert, near_expert)
-            ],
-            axis=0,
-        )
+            [jnp.where(place(meta_z, m, which), 1.0, 0.0) for which in (s, near)], axis=0
+        )
+
+    def complete(m):
+        for h in (0, 1):
+            for copy in forwarded[m, h]:
+                copy.wait_recv()
 
     def pick(m):
-        for copy in sent[m][2:] + forwarded[m]:
-            copy.wait_recv()
-        chooser = picking(m).astype(jnp.bfloat16)
-        for k in range(model // step):
-            columns = slice(k * step, (k + 1) * step)
-            rows_in = tok[:, planes[m], :, columns].reshape(lanes, step)
-            found = jnp.dot(chooser, rows_in, preferred_element_type=jnp.float32)
-            found = found.astype(xs.dtype)
-            xs[m, 0:slots, columns] = found[:slots]
-            xo[m, :, columns] = found[slots:]
+        chooser = picking(m)
+        lengths = inverse[planes[m]]
+        lengths = jnp.concatenate([lengths[0, 0:1], lengths[1, 0:1]], axis=1)
+        factor = jnp.sum(chooser * lengths, axis=1, keepdims=True)
+        chooser = chooser.astype(jnp.bfloat16)
+        for owner in range(4):
+            for k in range(width // step):
+                rows_in = tok[owner, planes[m], :, k * step : (k + 1) * step]
+                found = jnp.dot(chooser, rows_in, preferred_element_type=jnp.float32)
+                found = (found * factor).astype(xs.dtype)
+                columns = slice(owner * width + k * step, owner * width + (k + 1) * step)
+                xs[m, 0:slots, columns] = found[:slots]
+                xo[m, :, columns] = found[slots:]
         picks[m] = go(
             xo.at[m], xs.at[m, pl.ds(slots, slots)], xs_s.at[m], xs_r.at[m], n_dev
         )
@@ -374,8 +392,8 @@
     first_steps = (total_steps + 1) // 2
 
     def fall(m):
-        factor_mine = scale(meta_z, m, mine_expert)
-        factor_near = scale(meta_p, m, mine_expert)
+        factor_mine = scale(meta_z, m, s)
+        factor_near = scale(meta_p, m, s)
         wide = 512
 
         @pl.loop(0, model // wide)
@@ -392,10 +410,16 @@
     def expand(m):
         parts[m].wait_recv()
         spreader = picking(m).T.astype(jnp.bfloat16)
-        for k in range(model // step):
-            columns = slice(k * step, (k + 1) * step)
-            found = jnp.dot(spreader, po[m, :, columns], preferred_element_type=jnp.float32)
-            rt[m, :, :, columns] = found.astype(rt.dtype).reshape(4, tokens, step)
+        for owner in range(4):
+            holds = jnp.where(t == owner, 1.0, 0.0)
+            for k in range(width // step):
+                columns = slice(owner * width + k * step, owner * width + (k + 1) * step)
+                found = jnp.dot(spreader, po[m, :, columns], preferred_element_type=jnp.float32)
+                if m == 0:
+                    found += holds * proj[:, k * step : (k + 1) * step].astype(jnp.float32)
+                rt[m, :, :, columns] = found.astype(rt.dtype).reshape(4, tokens, step)
+
+    low, high = pl.ds(0, own // 2), pl.ds(own // 2, own // 2)
 
     def reduce_one(m):
         firsts[m] = (
@@ -426,78 +450,154 @@
         firsts[m][2].wait_recv()
         seconds[m][0].wait_recv()
         lower = wide_sum(rt[m, t, low], bx1[m, 0], by2[m])
+        if m:
+            sz[m, low] = lower.astype(sz.dtype)
+            lower_home = go(sz.at[m, low], zin.at[m, low], zbs.at[m, 0], zbr.at[m, 0], z_devs[m])
+        else:
+            home_sum[low] = lower
         firsts[m][3].wait_recv()
         seconds[m][1].wait_recv()
         upper = wide_sum(rt[m, t, high], by1[m, 0], bx2[m])
         if m:
-            sz[m, low] = lower.astype(sz.dtype)
             sz[m, high] = upper.astype(sz.dtype)
-            homes[m] = go(sz.at[m], zin.at[m], zbs.at[m], zbr.at[m], z_devs[m])
+            homes[m] = (
+                lower_home,
+                go(sz.at[m, high], zin.at[m, high], zbs.at[m, 1], zbr.at[m, 1], z_devs[m]),
+            )
         else:
-            home_sum[low] = lower
             home_sum[high] = upper
 
-    send(0)
-    forward(0)
+    def share_squares():
+        return [
+            go(squares, squares_in.at[t], qs.at[k], qr.at[k], device)
+            for k, device in enumerate((x_dev, y_dev, d_dev))
+        ]
+
+    def invert(square_copies):
+        for copy in square_copies:
+            copy.wait_recv()
+        total = (squares[...] + squares_in[tx]) + (squares_in[ty] + squares_in[td])
+        inverse[z] = lax.rsqrt(total * (1.0 / model) + EPS)
+        return {
+            m: go(inverse.at[z], inverse.at[z], qs.at[2 + m], qr.at[2 + m], z_devs[m])
+            for m in (1, 2, 3)
+        }
+
+    d_one.wait_recv()
+    sums = finish(0)
+    send(0, 0)
+    depart(0)
+    record(0, sums)
+    x_two.wait_recv()
+    acc[1] += product(1, tx)
+    d_two.wait_recv()
+    sums = finish(1)
+    send(0, 1)
+    depart(1)
+    record(1, sums)
+    square_copies = share_squares()
     for copy in meta_z_copies:
         copy.wait_recv()
     meta_near = go(meta_z, meta_p, ms.at[6], mr.at[6], n_dev)
-    send(1)
+    forward(0, 0)
+    arrive(1, 0)
+    relay(1, 0)
+    forward(0, 1)
+    arrive(1, 1)
+    relay(1, 1)
+    relay(3, 0, False)
+    relay(3, 1, False)
+    send(1, 0)
+    send(1, 1)
+    inverse_copies = invert(square_copies)
+    complete(0)
     pick(0)
+    arrive(2, 0)
+    relay(2, 0)
+    send(2, 0)
+    picks[0].wait_recv()
     for copy in loads[5:]:
         copy.wait()
-    picks[0].wait_recv()
     rise(0, 0, first_steps)
-    forward(1)
-    send(3)
+    arrive(2, 1)
+    relay(2, 1)
+    send(2, 1)
     rise(0, first_steps, total_steps)
     meta_near.wait_recv()
     fall(0)
+    forward(2, 0)
+    expand(0)
+    forward(2, 1)
+
+    @pl.when(outer)
+    def _():
+        arrive(3, 0)
+
+    send(3, 0)
+
+    @pl.when(outer)
+    def _():
+        arrive(3, 1)
+
+    send(3, 1)
+    complete(2)
+    inverse_copies[2].wait_recv()
+    pick(2)
+    forward(3, 0)
+    picks[2].wait_recv()
+    rise(2, 0, first_steps)
+    forward(3, 1)
+    forward(1, 0)
+    forward(1, 1)
+    rise(2, first_steps, total_steps)
+    fall(2)
+    complete(3)
+    inverse_copies[3].wait_recv()
+    pick(3)
+    expand(2)
+    reduce_one(2)
+    complete(1)
+    inverse_copies[1].wait_recv()
     pick(1)
+    picks[3].wait_recv()
+    rise(3, 0, first_steps)
+    rise(3, first_steps, total_steps)
+    reduce_two(2)
+    fall(3)
     picks[1].wait_recv()
     rise(1, 0, first_steps)
-    forward(3)
-    send(2)
-    rise(1, first_steps, total_steps)
-    fall(1)
-    pick(3)
-    picks[3].wait_recv()
-    rise(3, 0, first_steps)
-    forward(2)
-    rise(3, first_steps, total_steps)
-    fall(3)
     expand(3)
     reduce_one(3)
-    pick(2)
-    picks[2].wait_recv()
-    rise(2, 0, first_steps)
+    rise(1, first_steps, total_steps)
+    reduce_three(2)
+    fall(1)
     reduce_two(3)
-    rise(2, first_steps, total_steps)
-    fall(2)
-    expand(2)
-    reduce_one(2)
-    reduce_three(3)
     expand(1)
     reduce_one(1)
-    reduce_two(2)
-    expand(0)
+    reduce_three(3)
+    reduce_two(1)
     reduce_one(0)
-    reduce_three(2)
-    reduce_two(1)
     reduce_three(1)
     reduce_two(0)
     reduce_three(0)
-    for m in (3, 2, 1):
-        homes[m].wait_recv()
+    for m in (2, 3, 1):
+        homes[m][0].wait_recv()
+        homes[m][1].wait_recv()
     out_ref[...] = (
-        state[...] + (home_sum[...] + wide_sum(zin[1], zin[2], zin[3]))
+        res[...].astype(jnp.float32) + (home_sum[...] + wide_sum(zin[1], zin[2], zin[3]))
     ).astype(out_ref.dtype)
     for copy in copies:
         copy.wait_send()
     near_copy.wait_send()
-    to_x.wait_send()
-    to_y.wait_send()
-    to_d.wait_send()
+    for h in (0, 1):
+        out_one[h].wait_send()
+
+    @pl.when(inner)
+    def _():
+        for h in (0, 1):
+            out_three[h].wait_send()
+            for m in (1, 2, 3):
+                relay_copy(m, h).wait_send()
 
     @pl.when(has_far)
     def _():
@@ -531,11 +631,10 @@
             pltpu.VMEM((2 * rows, 2 * keys.shape[1]), kind),
             pltpu.VMEM(out_weight.shape, kind),
             pltpu.VMEM(residual.shape, kind),
+            pltpu.VMEM((4, tokens, width), kind),
             pltpu.VMEM((4, rows, depth), kind),
             pltpu.VMEM((2, rows // 2, width), jnp.float32),
             pltpu.VMEM((rows, width), kind),
-            pltpu.VMEM((4, rows // 4, width), kind),
-            pltpu.VMEM(residual.shape, jnp.float32),
             pltpu.VMEM(gate_weight.shape, kind),
             pltpu.VMEM(up_weight.shape, kind),
             pltpu.VMEM(down_weight.shape, kind),
@@ -543,7 +642,10 @@
             pltpu.VMEM((4, 2 * count, lanes), jnp.float32),
             pltpu.VMEM((4, 2 * count, lanes), jnp.float32),
             pltpu.VMEM((4, 2 * count, lanes), jnp.float32),
-            pltpu.VMEM((4, 4, tokens, model), kind),
+            pltpu.VMEM((2, 8, rows // 2), jnp.float32),
+            pltpu.VMEM((4, 2, 8, rows // 2), jnp.float32),
+            pltpu.VMEM((4, 2, 8, rows // 2), jnp.float32),
+            pltpu.VMEM((4, 4, rows, width), kind),
             pltpu.VMEM((4, 2 * slots, model), kind),
             pltpu.VMEM((4, slots, model), kind),
             pltpu.VMEM((2 * slots, gate_weight.shape[1]), kind),
@@ -559,22 +661,21 @@
             pltpu.VMEM((4, tokens, model), kind),
             pltpu.VMEM(residual.shape, jnp.float32),
             dma((8,)),
-            dma((2,)),
-            dma((2,)),
-            dma((6,)),
-            dma((6,)),
-            dma((3,)),
-            dma((3,)),
-            dma((7,)),
-            dma((7,)),
-            one, one, six, six, one, one, one, one, six, six, one, one,
+            dma((2,)), dma((2,)),
+            dma((6,)), dma((6,)),
+            dma((3,)), dma((3,)),
+            dma((7,)), dma((7,)),
+            dma((6,)), dma((6,)),
+            dma((7, 2)), dma((4, 2)),
+            dma((4, 8)), dma((4, 8)), one, one, one, one, six, six,
+            dma((4, 2)), dma((4, 2)),
         ],
         compiler_params=pltpu.CompilerParams(
             collective_id=0, has_side_effects=True, vmem_limit_bytes=60 * 1024 * 1024
         ),
     )(
         queries, keys, values, sink_logit, out_weight, residual, norm_gain.reshape(1, -1),
-        jnp.tile(routes.T, (1, 4)), jnp.tile(route_weights.T, (1, 4)),
+        routes.T, route_weights.T,
         gate_weight, up_weight, down_weight,
     )
 

time: 119 us -> 100 us (0.84)
  Pallas kernels: 115 us -> 98.2 us
  local copies, waits for them, and re-layouts: 4.34 us -> 1.67 us
    pallas_call x1, Pallas kernels: 115 us -> 98.2 us  [layer(): pl.pallas_call(layer_kernel, out_shape=jax.ShapeDtypeStruct(residual.shap...]
    another operation x4 -> x0, local copies, waits for them, and re-layouts: 2.67 us -> none  [the longest x2 1.34 us: layer(): jnp.tile(routes.T, (1, 4))]
where the time goes in v3:
time: 100 us; the launch traced here: 99.9 us
  Pallas kernels  98.2 us (98%)
  local copies, waits for them, and re-layouts  1.67 us (2%)
    pallas_call x1, Pallas kernels, layer(): pl.pallas_call(layer_kernel, out_shape=jax.ShapeDtypeStruct(residual.shap...  98.2 us

profile of v3, /device:TPU:0, one launch (start us, length us, event | category | flops | bytes accessed | tf_op | source)
XLA Modules:
  0.0 99.9 jit_solution(9654861622108196120)
XLA Ops:
  0.0 98.2 %shard_map.118 = bf16[64,2048]{1,0:T(8,128)(2,1)} custom-call(bf16[256,512]{1,0:T(8,128)(2,1)} %q_hbm.1, bf16[256,256]{1,0:T(8,128)(2,1)} %k_hbm.1, bf16[256,256]{1,0:T(8,128)(2,1)} %v_hbm.1, f32[8]{0:T(128)} %sink_ref.1, bf16[2048,512]{1,0:T(8,128)(2,1)} %w_hbm.1, bf16[64,2048]{1,0:T(8,128)(2,1)} %res_hbm.1, f32[1,2048]{1,0:T(1,128)} %bitcast.9, ...), custom_call_target="tpu_custom_call" | custom-call | tf_op jit(solution)/shard_map/pallas_call | solution.py:622
  98.2 1.7 %copy.14 = bf16[64,2048]{1,0:T(8,128)(2,1)} copy(bf16[64,2048]{1,0:T(8,128)(2,1)} %shard_map.118) | data formatting | bytes 524288

commit v4 on v3

--- a/solution.py
+++ b/solution.py
@@ -53,7 +53,7 @@
     meta, meta_in, meta_z, meta_p, squares, squares_in, inverse, tok, xs, xo, hidden, po, ps, rt,
     bx1, by1, bx2, by2, mid, sz, zin, home_sum,
     load, hs, hr, gs, gr, as_, ar, ms, mr, qs, qr, zs, zr, ds_, dr, xs_s, xs_r, ps_s, ps_r,
-    rs, rr, zbs, zbr,
+    rs, rr, zbs, zbr, hos, hor,
 ):
     s = lax.axis_index("sp")
     t, tx, ty, td = plane()
@@ -184,7 +184,7 @@
     band = jnp.abs(query + half - key) <= WINDOW
     upper = lax.broadcasted_iota(jnp.int32, (2 * half, 1), 0) < half
 
-    def attend(b):
+    def attend(b, first, end):
         valid = jnp.logical_and(
             band,
             jnp.logical_and(
@@ -194,7 +194,7 @@
         )
         keys_at = pl.ds(pl.multiple_of(b * half, half), span)
         mine = aligned(b * half, half)
-        for g in range(groups):
+        for g in range(first, end):
             pair = q[mine, 2 * g * HEAD : 2 * (g + 1) * HEAD]
             stacked = jnp.concatenate([pair[:, :HEAD], pair[:, HEAD:]], axis=0)
             scores = lax.dot_general(
@@ -220,23 +220,41 @@
     blocks = (1 - odd, odd)
     parts_of = [aligned(b * half, half) for b in blocks]
 
-    def spread(h, k):
-        piece = buf.at[t, parts_of[h]]
-        return (
+    wide_piece = depth // 2
+
+    def part(owner, h, j):
+        return buf.at[owner, parts_of[h], pl.ds(j * wide_piece, wide_piece)]
+
+    spreads, passes = {}, {}
+
+    def spread(h, j):
+        piece = part(t, h, j)
+        k = 4 * h + 2 * j
+        spreads[h, j] = (
             go(piece, piece, gs.at[k], gr.at[k], x_dev),
             go(piece, piece, gs.at[k + 1], gr.at[k + 1], y_dev),
         )
 
+    def hand_on(h, j):
+        spreads[h, j][j].wait_recv()
+        piece = part(ty if j else tx, h, j)
+        k = 8 + 2 * h + j
+        passes[h, j] = go(piece, piece, gs.at[k], gr.at[k], x_dev if j else y_dev)
+
     near_copy.wait_recv()
-    attend(blocks[0])
-    x_one, y_one = spread(0, 0)
+    attend(blocks[0], 0, groups // 2)
+    spread(0, 0)
+    attend(blocks[0], groups // 2, groups)
+    spread(0, 1)
 
     @pl.when(has_far)
     def _():
         far_copy.wait_recv()
 
-    attend(blocks[1])
-    x_two, y_two = spread(1, 2)
+    attend(blocks[1], 0, groups // 2)
+    spread(1, 0)
+    attend(blocks[1], groups // 2, groups)
+    spread(1, 1)
     for copy in meta_copies:
         copy.wait_recv()
     meta_z[z] = (meta[...] + meta_in[tx]) + (meta_in[ty] + meta_in[td])
@@ -244,25 +262,24 @@
         go(meta_z.at[z], meta_z.at[z], ms.at[2 + m], mr.at[2 + m], z_devs[m]) for m in (1, 2, 3)
     ]
     loads[3].wait()
-    for copy in res_copies:
-        copy.wait_recv()
 
     def product(h, owner):
         weight = w[pl.ds(pl.multiple_of(owner * depth, depth), depth)]
         return jnp.dot(buf[owner, parts_of[h]], weight, preferred_element_type=jnp.float32)
 
-    x_one.wait_recv()
-    piece = buf.at[tx, parts_of[0]]
-    d_one = go(piece, piece, gs.at[4], gr.at[4], y_dev)
-    acc[0] = product(0, t)
-    acc[0] += product(0, tx)
-    y_one.wait_recv()
-    acc[0] += product(0, ty)
-    y_two.wait_recv()
-    piece = buf.at[ty, parts_of[1]]
-    d_two = go(piece, piece, gs.at[5], gr.at[5], x_dev)
-    acc[1] = product(1, t)
-    acc[1] += product(1, ty)
+    def gather(h):
+        hand_on(h, 0)
+        acc[h] = product(h, t)
+        hand_on(h, 1)
+        spreads[h, 1][0].wait_recv()
+        acc[h] += product(h, tx)
+        spreads[h, 0][1].wait_recv()
+        acc[h] += product(h, ty)
+
+    gather(0)
+    for copy in res_copies:
+        copy.wait_recv()
+    gather(1)
     gain = gain_ref[:, aligned(t * width, width)]
 
     def finish(h):
@@ -356,10 +373,21 @@
             [jnp.where(place(meta_z, m, which), 1.0, 0.0) for which in (s, near)], axis=0
         )
 
+    handed = []
+
+    def hand_over():
+        for k, owner in enumerate((tx, ty, td)):
+            piece = tok.at[owner, z]
+            handed.append(go(piece, piece, hos.at[k], hor.at[k], z_devs[1]))
+
     def complete(m):
-        for h in (0, 1):
-            for copy in forwarded[m, h]:
+        if m == 1:
+            for copy in handed:
                 copy.wait_recv()
+        else:
+            for h in (0, 1):
+                for copy in forwarded[m, h]:
+                    copy.wait_recv()
 
     def pick(m):
         chooser = picking(m)
@@ -389,7 +417,6 @@
             hidden[:, columns] = (jax.nn.silu(g) * u).astype(hidden.dtype)
 
     total_steps = gate.shape[1] // step
-    first_steps = (total_steps + 1) // 2
 
     def fall(m):
         factor_mine = scale(meta_z, m, s)
@@ -421,13 +448,21 @@
 
     low, high = pl.ds(0, own // 2), pl.ds(own // 2, own // 2)
 
-    def reduce_one(m):
+    def reduce_far(m):
         firsts[m] = (
             go(rt.at[m, td, low], bx1.at[m, 1], rs.at[m, 0], rr.at[m, 0], x_dev),
             go(rt.at[m, td, high], by1.at[m, 1], rs.at[m, 1], rr.at[m, 1], y_dev),
+        )
+
+    def reduce_side(m):
+        firsts[m] += (
             go(rt.at[m, tx, low], bx1.at[m, 0], rs.at[m, 2], rr.at[m, 2], x_dev),
             go(rt.at[m, ty, high], by1.at[m, 0], rs.at[m, 3], rr.at[m, 3], y_dev),
         )
+
+    def reduce_one(m):
+        reduce_far(m)
+        reduce_side(m)
 
     def wide_sum(*pieces):
         result = pieces[0].astype(jnp.float32)
@@ -483,14 +518,14 @@
             for m in (1, 2, 3)
         }
 
-    d_one.wait_recv()
+    passes[0, 0].wait_recv()
+    passes[0, 1].wait_recv()
     sums = finish(0)
     send(0, 0)
     depart(0)
     record(0, sums)
-    x_two.wait_recv()
-    acc[1] += product(1, tx)
-    d_two.wait_recv()
+    passes[1, 0].wait_recv()
+    passes[1, 1].wait_recv()
     sums = finish(1)
     send(0, 1)
     depart(1)
@@ -507,8 +542,6 @@
     relay(1, 1)
     relay(3, 0, False)
     relay(3, 1, False)
-    send(1, 0)
-    send(1, 1)
     inverse_copies = invert(square_copies)
     complete(0)
     pick(0)
@@ -518,15 +551,15 @@
     picks[0].wait_recv()
     for copy in loads[5:]:
         copy.wait()
-    rise(0, 0, first_steps)
+    rise(0, 0, 2)
     arrive(2, 1)
     relay(2, 1)
     send(2, 1)
-    rise(0, first_steps, total_steps)
+    hand_over()
+    rise(0, 2, total_steps)
+    forward(2, 0)
     meta_near.wait_recv()
     fall(0)
-    forward(2, 0)
-    expand(0)
     forward(2, 1)
 
     @pl.when(outer)
@@ -534,6 +567,7 @@
         arrive(3, 0)
 
     send(3, 0)
+    expand(0)
 
     @pl.when(outer)
     def _():
@@ -545,30 +579,27 @@
     pick(2)
     forward(3, 0)
     picks[2].wait_recv()
-    rise(2, 0, first_steps)
+    rise(2, 0, total_steps - 1)
     forward(3, 1)
-    forward(1, 0)
-    forward(1, 1)
-    rise(2, first_steps, total_steps)
+    reduce_far(0)
+    rise(2, total_steps - 1, total_steps)
     fall(2)
     complete(3)
     inverse_copies[3].wait_recv()
     pick(3)
     expand(2)
     reduce_one(2)
+    picks[3].wait_recv()
+    rise(3, 0, total_steps)
+    fall(3)
+    reduce_two(2)
     complete(1)
     inverse_copies[1].wait_recv()
     pick(1)
-    picks[3].wait_recv()
-    rise(3, 0, first_steps)
-    rise(3, first_steps, total_steps)
-    reduce_two(2)
-    fall(3)
-    picks[1].wait_recv()
-    rise(1, 0, first_steps)
     expand(3)
     reduce_one(3)
-    rise(1, first_steps, total_steps)
+    picks[1].wait_recv()
+    rise(1, 0, total_steps)
     reduce_three(2)
     fall(1)
     reduce_two(3)
@@ -576,9 +607,9 @@
     reduce_one(1)
     reduce_three(3)
     reduce_two(1)
-    reduce_one(0)
+    reduce_side(0)
+    reduce_two(0)
     reduce_three(1)
-    reduce_two(0)
     reduce_three(0)
     for m in (2, 3, 1):
         homes[m][0].wait_recv()
@@ -621,7 +652,7 @@
     lanes = 4 * tokens
     return pl.pallas_call(
         layer_kernel,
-        out_shape=jax.ShapeDtypeStruct(residual.shape, kind),
+        out_shape=pltpu.VMEM(residual.shape, kind),
         in_specs=[anywhere] * 3
         + [pl.BlockSpec(memory_space=pltpu.SMEM), anywhere, anywhere, vmem, vmem, vmem]
         + [anywhere] * 3,
@@ -662,13 +693,13 @@
             pltpu.VMEM(residual.shape, jnp.float32),
             dma((8,)),
             dma((2,)), dma((2,)),
-            dma((6,)), dma((6,)),
+            dma((12,)), dma((12,)),
             dma((3,)), dma((3,)),
             dma((7,)), dma((7,)),
             dma((6,)), dma((6,)),
             dma((7, 2)), dma((4, 2)),
             dma((4, 8)), dma((4, 8)), one, one, one, one, six, six,
-            dma((4, 2)), dma((4, 2)),
+            dma((4, 2)), dma((4, 2)), dma((3,)), dma((3,)),
         ],
         compiler_params=pltpu.CompilerParams(
             collective_id=0, has_side_effects=True, vmem_limit_bytes=60 * 1024 * 1024

time: 100 us -> 93.3 us (0.933)
  Pallas kernels: 98.2 us -> 92.5 us
    pallas_call x1, Pallas kernels: 98.2 us -> 92.5 us  [layer(): pl.pallas_call(layer_kernel, out_shape=pltpu.VMEM(residual.shape, kind),...]
where the time goes in v4:
time: 93.3 us; the launch traced here: 93.2 us
  Pallas kernels  92.5 us (99%)
    pallas_call x1, Pallas kernels, layer(): pl.pallas_call(layer_kernel, out_shape=pltpu.VMEM(residual.shape, kind),...  92.5 us

profile of v4, /device:TPU:0, one launch (start us, length us, event | category | flops | bytes accessed | tf_op | source)
XLA Modules:
  0.0 93.2 jit_solution(4214152940246341022)
XLA Ops:
  0.0 92.5 %shard_map.118 = bf16[64,2048]{1,0:T(8,128)(2,1)S(1)} custom-call(bf16[256,512]{1,0:T(8,128)(2,1)} %q_hbm.1, bf16[256,256]{1,0:T(8,128)(2,1)} %k_hbm.1, bf16[256,256]{1,0:T(8,128)(2,1)} %v_hbm.1, f32[8]{0:T(128)} %sink_ref.1, bf16[2048,512]{1,0:T(8,128)(2,1)} %w_hbm.1, bf16[64,2048]{1,0:T(8,128)(2,1)} %res_hbm.1, f32[1,2048]{1,0:T(1,128)} %bitcast.9, ...), custom_call_target="tpu_custom_call" | custom-call | tf_op jit(solution)/shard_map/pallas_call | solution.py:653
  92.5 0.7 copy.14

commit v5 on v4

--- a/solution.py
+++ b/solution.py
@@ -47,9 +47,9 @@
 
 
 def layer_kernel(
-    q_hbm, k_hbm, v_hbm, sink_ref, w_hbm, res_hbm, gain_ref, routes_ref, route_weights_ref,
+    q_hbm, k_hbm, v_hbm, sink_hbm, w_hbm, res_hbm, gain_hbm, routes_hbm, route_weights_hbm,
     gate_hbm, up_hbm, down_hbm, out_ref,
-    q, kv, w, res, res_in, buf, acc, proj, gate, up, down,
+    sink_ref, gain_ref, routes_ref, route_weights_ref, q, kv, w, res, res_in, buf, acc, proj, gate, up, down,
     meta, meta_in, meta_z, meta_p, squares, squares_in, inverse, tok, xs, xo, hidden, po, ps, rt,
     bx1, by1, bx2, by2, mid, sz, zin, home_sum,
     load, hs, hr, gs, gr, as_, ar, ms, mr, qs, qr, zs, zr, ds_, dr, xs_s, xs_r, ps_s, ps_r,
@@ -85,11 +85,13 @@
                 (gate_hbm, gate),
                 (up_hbm, up),
                 (down_hbm, down),
+                (sink_hbm, sink_ref),
+                (routes_hbm, routes_ref),
+                (route_weights_hbm, route_weights_ref),
+                (gain_hbm, gain_ref),
             )
         )
     ]
-    for copy in loads[:5]:
-        copy.start()
     barrier = pltpu.get_barrier_semaphore()
     for device in [x_dev, y_dev, d_dev, n_dev] + z_devs[1:]:
         pl.semaphore_signal(barrier, inc=1, device_id=device, device_id_type=MESH)
@@ -97,6 +99,12 @@
     @pl.when(has_far)
     def _():
         pl.semaphore_signal(barrier, inc=1, device_id=f_dev, device_id_type=MESH)
+
+    for copy in loads[:5] + loads[8:]:
+        copy.start()
+
+    @pl.when(has_far)
+    def _():
         pl.semaphore_wait(barrier, 8)
 
     @pl.when(jnp.logical_not(has_far))
@@ -147,6 +155,8 @@
     expert = lax.broadcasted_iota(jnp.int32, (count, lanes), 0)
     lane = lax.broadcasted_iota(jnp.int32, (count, lanes), 1)
     mine_lane = jnp.logical_and(lane >= t * tokens, lane < (t + 1) * tokens)
+    for copy in loads[8:]:
+        copy.wait()
     routes = jnp.concatenate([routes_ref[...]] * 4, axis=1)
     route_weights = jnp.concatenate([route_weights_ref[...]] * 4, axis=1)
     hit_one = routes[0:1, :] == expert
@@ -169,7 +179,7 @@
         for k, device in enumerate((x_dev, y_dev, d_dev))
     ]
 
-    for copy in loads[5:]:
+    for copy in loads[5:8]:
         copy.start()
 
     @pl.when(jnp.logical_not(has_far))
@@ -403,9 +413,19 @@
                 columns = slice(owner * width + k * step, owner * width + (k + 1) * step)
                 xs[m, 0:slots, columns] = found[:slots]
                 xo[m, :, columns] = found[slots:]
-        picks[m] = go(
-            xo.at[m], xs.at[m, pl.ds(slots, slots)], xs_s.at[m], xs_r.at[m], n_dev
-        )
+            if owner % 2:
+                columns = pl.ds((owner - 1) * width, 2 * width)
+                picks[m, owner // 2] = go(
+                    xo.at[m, :, columns],
+                    xs.at[m, pl.ds(slots, slots), columns],
+                    xs_s.at[m, owner // 2],
+                    xs_r.at[m, owner // 2],
+                    n_dev,
+                )
+
+    def picked(m):
+        for k in (0, 1):
+            picks[m, k].wait_recv()
 
     def rise(m, begin, end):
         @pl.loop(begin, end)
@@ -423,21 +443,29 @@
         factor_near = scale(meta_p, m, s)
         wide = 512
 
-        @pl.loop(0, model // wide)
-        def _(k):
-            columns = pl.ds(pl.multiple_of(k * wide, wide), wide)
-            share = jnp.dot(hidden[...], down[:, columns], preferred_element_type=jnp.float32)
-            po[m, 0:slots, columns] = (share[:slots] * factor_mine).astype(po.dtype)
-            ps[m, :, columns] = (share[slots:] * factor_near).astype(ps.dtype)
-
-        parts[m] = go(
-            ps.at[m], po.at[m, pl.ds(slots, slots)], ps_s.at[m], ps_r.at[m], n_dev
-        )
+        for side in (0, 1):
+
+            @pl.loop(side * model // (2 * wide), (side + 1) * model // (2 * wide))
+            def _(k):
+                columns = pl.ds(pl.multiple_of(k * wide, wide), wide)
+                share = jnp.dot(hidden[...], down[:, columns], preferred_element_type=jnp.float32)
+                po[m, 0:slots, columns] = (share[:slots] * factor_mine).astype(po.dtype)
+                ps[m, :, columns] = (share[slots:] * factor_near).astype(ps.dtype)
+
+            columns = pl.ds(side * (model // 2), model // 2)
+            parts[m, side] = go(
+                ps.at[m, :, columns],
+                po.at[m, pl.ds(slots, slots), columns],
+                ps_s.at[m, side],
+                ps_r.at[m, side],
+                n_dev,
+            )
 
     def expand(m):
-        parts[m].wait_recv()
         spreader = picking(m).T.astype(jnp.bfloat16)
         for owner in range(4):
+            if owner % 2 == 0:
+                parts[m, owner // 2].wait_recv()
             holds = jnp.where(t == owner, 1.0, 0.0)
             for k in range(width // step):
                 columns = slice(owner * width + k * step, owner * width + (k + 1) * step)
@@ -448,16 +476,35 @@
 
     low, high = pl.ds(0, own // 2), pl.ds(own // 2, own // 2)
 
-    def reduce_far(m):
-        firsts[m] = (
-            go(rt.at[m, td, low], bx1.at[m, 1], rs.at[m, 0], rr.at[m, 0], x_dev),
-            go(rt.at[m, td, high], by1.at[m, 1], rs.at[m, 1], rr.at[m, 1], y_dev),
-        )
-
-    def reduce_side(m):
-        firsts[m] += (
-            go(rt.at[m, tx, low], bx1.at[m, 0], rs.at[m, 2], rr.at[m, 2], x_dev),
-            go(rt.at[m, ty, high], by1.at[m, 0], rs.at[m, 3], rr.at[m, 3], y_dev),
+    def side_of(m, c):
+        if c is None:
+            return m, pl.ds(0, model)
+        return m if c == 0 else {1: 4, 0: 5, 3: 6}[m], pl.ds(c * (model // 2), model // 2)
+
+    def reduce_far(m, c=None):
+        k, columns = side_of(m, c)
+        firsts[m, c] = (
+            go(
+                rt.at[m, td, low, columns], bx1.at[m, 1, :, columns],
+                rs.at[k, 0], rr.at[k, 0], x_dev,
+            ),
+            go(
+                rt.at[m, td, high, columns], by1.at[m, 1, :, columns],
+                rs.at[k, 1], rr.at[k, 1], y_dev,
+            ),
+        )
+
+    def reduce_side(m, c=None):
+        k, columns = side_of(m, c)
+        firsts[m, c] += (
+            go(
+                rt.at[m, tx, low, columns], bx1.at[m, 0, :, columns],
+                rs.at[k, 2], rr.at[k, 2], x_dev,
+            ),
+            go(
+                rt.at[m, ty, high, columns], by1.at[m, 0, :, columns],
+                rs.at[k, 3], rr.at[k, 3], y_dev,
+            ),
         )
 
     def reduce_one(m):
@@ -470,37 +517,68 @@
             result = result + piece.astype(jnp.float32)
         return result
 
-    def reduce_two(m):
-        firsts[m][0].wait_recv()
-        mid[m, 0] = wide_sum(rt[m, ty, low], bx1[m, 1]).astype(mid.dtype)
-        to_side = go(mid.at[m, 0], by2.at[m], rs.at[m, 4], rr.at[m, 4], y_dev)
-        firsts[m][1].wait_recv()
-        mid[m, 1] = wide_sum(rt[m, tx, high], by1[m, 1]).astype(mid.dtype)
-        seconds[m] = (
+    def reduce_two(m, c=None):
+        k, columns = side_of(m, c)
+        firsts[m, c][0].wait_recv()
+        mid[m, 0, :, columns] = wide_sum(
+            rt[m, ty, low, columns], bx1[m, 1, :, columns]
+        ).astype(mid.dtype)
+        to_side = go(
+            mid.at[m, 0, :, columns], by2.at[m, :, columns], rs.at[k, 4], rr.at[k, 4], y_dev
+        )
+        firsts[m, c][1].wait_recv()
+        mid[m, 1, :, columns] = wide_sum(
+            rt[m, tx, high, columns], by1[m, 1, :, columns]
+        ).astype(mid.dtype)
+        seconds[m, c] = (
             to_side,
-            go(mid.at[m, 1], bx2.at[m], rs.at[m, 5], rr.at[m, 5], x_dev),
-        )
-
-    def reduce_three(m):
-        firsts[m][2].wait_recv()
-        seconds[m][0].wait_recv()
-        lower = wide_sum(rt[m, t, low], bx1[m, 0], by2[m])
-        if m:
-            sz[m, low] = lower.astype(sz.dtype)
-            lower_home = go(sz.at[m, low], zin.at[m, low], zbs.at[m, 0], zbr.at[m, 0], z_devs[m])
-        else:
-            home_sum[low] = lower
-        firsts[m][3].wait_recv()
-        seconds[m][1].wait_recv()
-        upper = wide_sum(rt[m, t, high], by1[m, 0], bx2[m])
-        if m:
-            sz[m, high] = upper.astype(sz.dtype)
-            homes[m] = (
-                lower_home,
-                go(sz.at[m, high], zin.at[m, high], zbs.at[m, 1], zbr.at[m, 1], z_devs[m]),
+            go(mid.at[m, 1, :, columns], bx2.at[m, :, columns], rs.at[k, 5], rr.at[k, 5], x_dev),
+        )
+
+    home_two = (jnp.where(inner, z_devs[2][0], z_devs[1][0]), t)
+
+    def reduce_three(m, c=None):
+        k, columns = side_of(m, c)
+
+        def home(rows_at, value, h):
+            if m == 0:
+                home_sum[rows_at, columns] += value
+                return None
+            if m == 3:
+
+                @pl.when(inner)
+                def _():
+                    if not c:
+                        homes[2, None][h].wait_recv()
+                    joint = value + zin[2, rows_at, columns].astype(jnp.float32)
+                    sz[m, rows_at, columns] = joint.astype(sz.dtype)
+
+                @pl.when(outer)
+                def _():
+                    sz[m, rows_at, columns] = value.astype(sz.dtype)
+
+            else:
+                sz[m, rows_at, columns] = value.astype(sz.dtype)
+            return go(
+                sz.at[m, rows_at, columns], zin.at[m, rows_at, columns],
+                zbs.at[k, h], zbr.at[k, h], home_two if m == 2 else z_devs[m],
             )
-        else:
-            home_sum[high] = upper
+
+        firsts[m, c][2].wait_recv()
+        seconds[m, c][0].wait_recv()
+        lower = home(
+            low,
+            wide_sum(rt[m, t, low, columns], bx1[m, 0, :, columns], by2[m, :, columns]),
+            0,
+        )
+        firsts[m, c][3].wait_recv()
+        seconds[m, c][1].wait_recv()
+        upper = home(
+            high,
+            wide_sum(rt[m, t, high, columns], by1[m, 0, :, columns], bx2[m, :, columns]),
+            1,
+        )
+        homes[m, c] = (lower, upper)
 
     def share_squares():
         return [
@@ -537,87 +615,95 @@
     forward(0, 0)
     arrive(1, 0)
     relay(1, 0)
+    relay(3, 0, False)
     forward(0, 1)
     arrive(1, 1)
     relay(1, 1)
-    relay(3, 0, False)
     relay(3, 1, False)
     inverse_copies = invert(square_copies)
-    complete(0)
-    pick(0)
     arrive(2, 0)
     relay(2, 0)
     send(2, 0)
-    picks[0].wait_recv()
-    for copy in loads[5:]:
-        copy.wait()
-    rise(0, 0, 2)
+    complete(0)
+    pick(0)
     arrive(2, 1)
     relay(2, 1)
     send(2, 1)
     hand_over()
+    picked(0)
+    for copy in loads[5:8]:
+        copy.wait()
+    rise(0, 0, 2)
+    forward(2, 0)
     rise(0, 2, total_steps)
-    forward(2, 0)
+    forward(2, 1)
+
+    @pl.when(outer)
+    def _():
+        arrive(3, 0)
+
+    send(3, 0)
     meta_near.wait_recv()
     fall(0)
-    forward(2, 1)
 
     @pl.when(outer)
     def _():
-        arrive(3, 0)
-
-    send(3, 0)
+        arrive(3, 1)
+
+    send(3, 1)
     expand(0)
-
-    @pl.when(outer)
-    def _():
-        arrive(3, 1)
-
-    send(3, 1)
     complete(2)
     inverse_copies[2].wait_recv()
     pick(2)
+    picked(2)
+    rise(2, 0, 2)
     forward(3, 0)
-    picks[2].wait_recv()
-    rise(2, 0, total_steps - 1)
+    rise(2, 2, total_steps)
     forward(3, 1)
-    reduce_far(0)
-    rise(2, total_steps - 1, total_steps)
+    reduce_far(0, 0)
+    reduce_far(0, 1)
     fall(2)
     complete(3)
     inverse_copies[3].wait_recv()
     pick(3)
     expand(2)
     reduce_one(2)
-    picks[3].wait_recv()
+    picked(3)
     rise(3, 0, total_steps)
+    reduce_two(2)
+    reduce_side(0, 0)
     fall(3)
-    reduce_two(2)
     complete(1)
     inverse_copies[1].wait_recv()
     pick(1)
     expand(3)
-    reduce_one(3)
-    picks[1].wait_recv()
-    rise(1, 0, total_steps)
+    reduce_far(3, 0)
+    reduce_side(3, 0)
+    reduce_far(3, 1)
+    picked(1)
+    rise(1, 0, 1)
     reduce_three(2)
+    rise(1, 1, total_steps - 1)
+    reduce_two(3, 0)
+    reduce_side(3, 1)
+    rise(1, total_steps - 1, total_steps)
     fall(1)
-    reduce_two(3)
+    reduce_two(3, 1)
+    drained = len(copies)
     expand(1)
-    reduce_one(1)
-    reduce_three(3)
-    reduce_two(1)
-    reduce_side(0)
-    reduce_two(0)
-    reduce_three(1)
-    reduce_three(0)
-    for m in (2, 3, 1):
-        homes[m][0].wait_recv()
-        homes[m][1].wait_recv()
-    out_ref[...] = (
-        res[...].astype(jnp.float32) + (home_sum[...] + wide_sum(zin[1], zin[2], zin[3]))
-    ).astype(out_ref.dtype)
-    for copy in copies:
+    reduce_far(1, 0)
+    reduce_side(1, 0)
+    reduce_far(1, 1)
+    reduce_three(3, 0)
+    reduce_three(3, 1)
+    reduce_two(1, 0)
+    reduce_side(1, 1)
+    reduce_two(1, 1)
+    reduce_side(0, 1)
+    reduce_two(0, 0)
+    reduce_two(0, 1)
+    reduce_three(1, 0)
+    for copy in copies[: drained - 8]:
         copy.wait_send()
     near_copy.wait_send()
     for h in (0, 1):
@@ -633,6 +719,28 @@
     @pl.when(has_far)
     def _():
         far_copy.wait_send()
+
+    reduce_three(1, 1)
+    @pl.when(outer)
+    def _():
+        for copy in homes[2, None]:
+            copy.wait_recv()
+
+    for copy in homes[3, 0] + homes[3, 1]:
+        copy.wait_recv()
+    home_sum[...] = (
+        res[...].astype(jnp.float32)
+        + jnp.where(outer, zin[2].astype(jnp.float32), 0.0)
+        + zin[3].astype(jnp.float32)
+    )
+    reduce_three(0, 0)
+    reduce_three(0, 1)
+    for c in (0, 1):
+        for copy in homes[1, c]:
+            copy.wait_recv()
+    out_ref[...] = (home_sum[...] + zin[1].astype(jnp.float32)).astype(out_ref.dtype)
+    for copy in copies[drained - 8 :]:
+        copy.wait_send()
 
 
 def layer(
@@ -648,16 +756,18 @@
     anywhere = pl.BlockSpec(memory_space=pl.ANY)
     vmem = pl.BlockSpec(memory_space=pltpu.VMEM)
     dma = pltpu.SemaphoreType.DMA
-    one, six = dma((4,)), dma((4, 6))
+    two = dma((4, 2))
     lanes = 4 * tokens
     return pl.pallas_call(
         layer_kernel,
         out_shape=pltpu.VMEM(residual.shape, kind),
-        in_specs=[anywhere] * 3
-        + [pl.BlockSpec(memory_space=pltpu.SMEM), anywhere, anywhere, vmem, vmem, vmem]
-        + [anywhere] * 3,
+        in_specs=[anywhere] * 12,
         out_specs=vmem,
         scratch_shapes=[
+            pltpu.SMEM(sink_logit.shape, jnp.float32),
+            pltpu.VMEM((1, model), jnp.float32),
+            pltpu.VMEM((2, tokens), jnp.int32),
+            pltpu.VMEM((2, tokens), jnp.float32),
             pltpu.VMEM(queries.shape, kind),
             pltpu.VMEM((2 * rows, 2 * keys.shape[1]), kind),
             pltpu.VMEM(out_weight.shape, kind),
@@ -691,15 +801,15 @@
             pltpu.VMEM((4, tokens, model), kind),
             pltpu.VMEM((4, tokens, model), kind),
             pltpu.VMEM(residual.shape, jnp.float32),
-            dma((8,)),
+            dma((12,)),
             dma((2,)), dma((2,)),
             dma((12,)), dma((12,)),
             dma((3,)), dma((3,)),
             dma((7,)), dma((7,)),
             dma((6,)), dma((6,)),
             dma((7, 2)), dma((4, 2)),
-            dma((4, 8)), dma((4, 8)), one, one, one, one, six, six,
-            dma((4, 2)), dma((4, 2)), dma((3,)), dma((3,)),
+            dma((4, 8)), dma((4, 8)), two, two, two, two, dma((7, 6)), dma((7, 6)),
+            dma((7, 2)), dma((7, 2)), dma((3,)), dma((3,)),
         ],
         compiler_params=pltpu.CompilerParams(
             collective_id=0, has_side_effects=True, vmem_limit_bytes=60 * 1024 * 1024

time: 93.3 us -> 87.8 us (0.941)
  Pallas kernels: 92.5 us -> 87 us
    pallas_call x1, Pallas kernels: 92.5 us -> 87 us  [layer(): pl.pallas_call(layer_kernel, out_shape=pltpu.VMEM(residual.shape, kind),...]
where the time goes in v5:
time: 87.8 us; the launch traced here: 87.7 us
  Pallas kernels  87 us (99%)
    pallas_call x1, Pallas kernels, layer(): pl.pallas_call(layer_kernel, out_shape=pltpu.VMEM(residual.shape, kind),...  87 us

profile of v5, /device:TPU:0, one launch (start us, length us, event | category | flops | bytes accessed | tf_op | source)
XLA Modules:
  0.0 87.7 jit_solution(13075529732626473613)
XLA Ops:
  0.0 87.0 %shard_map.118 = bf16[64,2048]{1,0:T(8,128)(2,1)S(1)} custom-call(bf16[256,512]{1,0:T(8,128)(2,1)} %q_hbm.1, bf16[256,256]{1,0:T(8,128)(2,1)} %k_hbm.1, bf16[256,256]{1,0:T(8,128)(2,1)} %v_hbm.1, f32[8]{0:T(128)} %sink_hbm.1, bf16[2048,512]{1,0:T(8,128)(2,1)} %w_hbm.1, bf16[64,2048]{1,0:T(8,128)(2,1)} %res_hbm.1, f32[1,2048]{1,0:T(1,128)} %bitcast.9, ...), custom_call_target="tpu_custom_call" | custom-call | tf_op jit(solution)/shard_map/pallas_call | solution.py:761
  87.0 0.7 copy.14

commit v6 on v5

--- a/solution.py
+++ b/solution.py
@@ -1,4 +1,4 @@
-import functools
+import math
 
 import jax
 import jax.numpy as jnp
@@ -52,8 +52,7 @@
     sink_ref, gain_ref, routes_ref, route_weights_ref, q, kv, w, res, res_in, buf, acc, proj, gate, up, down,
     meta, meta_in, meta_z, meta_p, squares, squares_in, inverse, tok, xs, xo, hidden, po, ps, rt,
     bx1, by1, bx2, by2, mid, sz, zin, home_sum,
-    load, hs, hr, gs, gr, as_, ar, ms, mr, qs, qr, zs, zr, ds_, dr, xs_s, xs_r, ps_s, ps_r,
-    rs, rr, zbs, zbr, hos, hor,
+    load, sends, hs, hr, gr, ar, mr, qr, zs, zr, dr, xs_r, ps_r, rr, zbr, hor,
 ):
     s = lax.axis_index("sp")
     t, tx, ty, td = plane()
@@ -128,13 +127,22 @@
         far_copy.start()
 
     near_copy.start()
-    copies = []
-
-    def go(*args):
-        copy = remote(*args)
+    amounts = [0] * sends.shape[0]
+
+    def go(source, target, group, recv, device):
+        copy = remote(source, target, sends.at[group], recv, device)
         copy.start()
-        copies.append(copy)
+        amounts[group] += math.prod(source.shape) * source.dtype.itemsize
         return copy
+
+    def settle(group):
+        line = tok.shape[3] * tok.dtype.itemsize
+        lines = amounts[group] // line
+        if lines <= tok.shape[2]:
+            whole = tok.at[0, 0, pl.ds(0, lines)]
+        else:
+            whole = tok.at[0, pl.ds(0, lines // tok.shape[2])]
+        remote(whole, whole, sends.at[group], hr.at[0], x_dev).wait_send()
 
     own, model = res.shape
     width = w.shape[1]
@@ -143,7 +151,7 @@
         go(
             res.at[:, aligned(owner * width, width)],
             res_in.at[t],
-            as_.at[k],
+            1,
             ar.at[k],
             device,
         )
@@ -175,7 +183,7 @@
         hit_one, route_weights[0:1, :], route_weights[1:2, :]
     )
     meta_copies = [
-        go(meta, meta_in.at[t], ms.at[k], mr.at[k], device)
+        go(meta, meta_in.at[t], 2, mr.at[k], device)
         for k, device in enumerate((x_dev, y_dev, d_dev))
     ]
 
@@ -241,15 +249,15 @@
         piece = part(t, h, j)
         k = 4 * h + 2 * j
         spreads[h, j] = (
-            go(piece, piece, gs.at[k], gr.at[k], x_dev),
-            go(piece, piece, gs.at[k + 1], gr.at[k + 1], y_dev),
+            go(piece, piece, 0, gr.at[k], x_dev),
+            go(piece, piece, 0, gr.at[k + 1], y_dev),
         )
 
     def hand_on(h, j):
         spreads[h, j][j].wait_recv()
         piece = part(ty if j else tx, h, j)
         k = 8 + 2 * h + j
-        passes[h, j] = go(piece, piece, gs.at[k], gr.at[k], x_dev if j else y_dev)
+        passes[h, j] = go(piece, piece, 0, gr.at[k], x_dev if j else y_dev)
 
     near_copy.wait_recv()
     attend(blocks[0], 0, groups // 2)
@@ -269,7 +277,7 @@
         copy.wait_recv()
     meta_z[z] = (meta[...] + meta_in[tx]) + (meta_in[ty] + meta_in[td])
     meta_z_copies = [
-        go(meta_z.at[z], meta_z.at[z], ms.at[2 + m], mr.at[2 + m], z_devs[m]) for m in (1, 2, 3)
+        go(meta_z.at[z], meta_z.at[z], 2, mr.at[2 + m], z_devs[m]) for m in (1, 2, 3)
     ]
     loads[3].wait()
 
@@ -331,7 +339,7 @@
         def _():
             out_three[h].start()
 
-    sent, forwarded, picks, parts, firsts, seconds, homes = {}, {}, {}, {}, {}, {}, {}
+    sent, parts, firsts, seconds, homes = {}, {}, {}, {}, {}
 
     def arrive(m, h):
         z_in[m, h].wait_recv()
@@ -345,19 +353,20 @@
 
     def send(m, h):
         piece = tok.at[t, planes[m], parts_of[h]]
+        k = max(m - 1, 0)
         sent[m, h] = (
-            go(piece, piece, ds_.at[m, 2 * h], dr.at[m, 2 * h], x_dev),
-            go(piece, piece, ds_.at[m, 2 * h + 1], dr.at[m, 2 * h + 1], y_dev),
+            go(piece, piece, 5 + k, dr.at[k, 2 * h], x_dev),
+            go(piece, piece, 5 + k, dr.at[k, 2 * h + 1], y_dev),
         )
 
     def forward(m, h):
+        k = max(m - 1, 0)
         sent[m, h][0].wait_recv()
         piece = tok.at[tx, planes[m], aligned(blocks[h] * half, half // 2)]
-        first = go(piece, piece, ds_.at[m, 4 + 2 * h], dr.at[m, 4 + 2 * h], y_dev)
+        go(piece, piece, 5 + k, dr.at[k, 4], y_dev)
         sent[m, h][1].wait_recv()
         piece = tok.at[ty, planes[m], aligned(blocks[h] * half + half // 2, half // 2)]
-        second = go(piece, piece, ds_.at[m, 5 + 2 * h], dr.at[m, 5 + 2 * h], x_dev)
-        forwarded[m, h] = (first, second)
+        go(piece, piece, 5 + k, dr.at[k, 4], x_dev)
 
     slots = xo.shape[1]
     capacity = slots // 4
@@ -383,21 +392,17 @@
             [jnp.where(place(meta_z, m, which), 1.0, 0.0) for which in (s, near)], axis=0
         )
 
-    handed = []
-
     def hand_over():
         for k, owner in enumerate((tx, ty, td)):
             piece = tok.at[owner, z]
-            handed.append(go(piece, piece, hos.at[k], hor.at[k], z_devs[1]))
+            go(piece, piece, 4, hor, z_devs[1])
 
     def complete(m):
         if m == 1:
-            for copy in handed:
-                copy.wait_recv()
+            whole, recv = tok.at[0, pl.ds(0, 3)], hor
         else:
-            for h in (0, 1):
-                for copy in forwarded[m, h]:
-                    copy.wait_recv()
+            whole, recv = tok.at[0, 0], dr.at[max(m - 1, 0), 4]
+        remote(whole, whole, sends.at[4], recv, x_dev).wait_recv()
 
     def pick(m):
         chooser = picking(m)
@@ -415,17 +420,17 @@
                 xo[m, :, columns] = found[slots:]
             if owner % 2:
                 columns = pl.ds((owner - 1) * width, 2 * width)
-                picks[m, owner // 2] = go(
+                go(
                     xo.at[m, :, columns],
                     xs.at[m, pl.ds(slots, slots), columns],
-                    xs_s.at[m, owner // 2],
-                    xs_r.at[m, owner // 2],
+                    8 + m,
+                    xs_r.at[m],
                     n_dev,
                 )
 
     def picked(m):
-        for k in (0, 1):
-            picks[m, k].wait_recv()
+        whole = xo.at[m]
+        remote(whole, whole, sends.at[8 + m], xs_r.at[m], n_dev).wait_recv()
 
     def rise(m, begin, end):
         @pl.loop(begin, end)
@@ -456,7 +461,7 @@
             parts[m, side] = go(
                 ps.at[m, :, columns],
                 po.at[m, pl.ds(slots, slots), columns],
-                ps_s.at[m, side],
+                12 + m,
                 ps_r.at[m, side],
                 n_dev,
             )
@@ -486,11 +491,11 @@
         firsts[m, c] = (
             go(
                 rt.at[m, td, low, columns], bx1.at[m, 1, :, columns],
-                rs.at[k, 0], rr.at[k, 0], x_dev,
+                16 + m, rr.at[k, 0], x_dev,
             ),
             go(
                 rt.at[m, td, high, columns], by1.at[m, 1, :, columns],
-                rs.at[k, 1], rr.at[k, 1], y_dev,
+                16 + m, rr.at[k, 1], y_dev,
             ),
         )
 
@@ -499,11 +504,11 @@
         firsts[m, c] += (
             go(
                 rt.at[m, tx, low, columns], bx1.at[m, 0, :, columns],
-                rs.at[k, 2], rr.at[k, 2], x_dev,
+                16 + m, rr.at[k, 2], x_dev,
             ),
             go(
                 rt.at[m, ty, high, columns], by1.at[m, 0, :, columns],
-                rs.at[k, 3], rr.at[k, 3], y_dev,
+                16 + m, rr.at[k, 3], y_dev,
             ),
         )
 
@@ -524,7 +529,7 @@
             rt[m, ty, low, columns], bx1[m, 1, :, columns]
         ).astype(mid.dtype)
         to_side = go(
-            mid.at[m, 0, :, columns], by2.at[m, :, columns], rs.at[k, 4], rr.at[k, 4], y_dev
+            mid.at[m, 0, :, columns], by2.at[m, :, columns], 16 + m, rr.at[k, 4], y_dev
         )
         firsts[m, c][1].wait_recv()
         mid[m, 1, :, columns] = wide_sum(
@@ -532,7 +537,7 @@
         ).astype(mid.dtype)
         seconds[m, c] = (
             to_side,
-            go(mid.at[m, 1, :, columns], bx2.at[m, :, columns], rs.at[k, 5], rr.at[k, 5], x_dev),
+            go(mid.at[m, 1, :, columns], bx2.at[m, :, columns], 16 + m, rr.at[k, 5], x_dev),
         )
 
     home_two = (jnp.where(inner, z_devs[2][0], z_devs[1][0]), t)
@@ -561,7 +566,7 @@
                 sz[m, rows_at, columns] = value.astype(sz.dtype)
             return go(
                 sz.at[m, rows_at, columns], zin.at[m, rows_at, columns],
-                zbs.at[k, h], zbr.at[k, h], home_two if m == 2 else z_devs[m],
+                20 + m, zbr.at[k, h], home_two if m == 2 else z_devs[m],
             )
 
         firsts[m, c][2].wait_recv()
@@ -582,7 +587,7 @@
 
     def share_squares():
         return [
-            go(squares, squares_in.at[t], qs.at[k], qr.at[k], device)
+            go(squares, squares_in.at[t], 3, qr.at[k], device)
             for k, device in enumerate((x_dev, y_dev, d_dev))
         ]
 
@@ -592,7 +597,7 @@
         total = (squares[...] + squares_in[tx]) + (squares_in[ty] + squares_in[td])
         inverse[z] = lax.rsqrt(total * (1.0 / model) + EPS)
         return {
-            m: go(inverse.at[z], inverse.at[z], qs.at[2 + m], qr.at[2 + m], z_devs[m])
+            m: go(inverse.at[z], inverse.at[z], 3, qr.at[2 + m], z_devs[m])
             for m in (1, 2, 3)
         }
 
@@ -611,7 +616,7 @@
     square_copies = share_squares()
     for copy in meta_z_copies:
         copy.wait_recv()
-    meta_near = go(meta_z, meta_p, ms.at[6], mr.at[6], n_dev)
+    meta_near = go(meta_z, meta_p, 2, mr.at[6], n_dev)
     forward(0, 0)
     arrive(1, 0)
     relay(1, 0)
@@ -689,7 +694,6 @@
     rise(1, total_steps - 1, total_steps)
     fall(1)
     reduce_two(3, 1)
-    drained = len(copies)
     expand(1)
     reduce_far(1, 0)
     reduce_side(1, 0)
@@ -703,8 +707,9 @@
     reduce_two(0, 0)
     reduce_two(0, 1)
     reduce_three(1, 0)
-    for copy in copies[: drained - 8]:
-        copy.wait_send()
+    for group in range(24):
+        if group not in (16, 17, 19, 20, 21, 23):
+            settle(group)
     near_copy.wait_send()
     for h in (0, 1):
         out_one[h].wait_send()
@@ -739,8 +744,8 @@
         for copy in homes[1, c]:
             copy.wait_recv()
     out_ref[...] = (home_sum[...] + zin[1].astype(jnp.float32)).astype(out_ref.dtype)
-    for copy in copies[drained - 8 :]:
-        copy.wait_send()
+    for group in (16, 17, 19, 21, 23):
+        settle(group)
 
 
 def layer(
@@ -756,7 +761,6 @@
     anywhere = pl.BlockSpec(memory_space=pl.ANY)
     vmem = pl.BlockSpec(memory_space=pltpu.VMEM)
     dma = pltpu.SemaphoreType.DMA
-    two = dma((4, 2))
     lanes = 4 * tokens
     return pl.pallas_call(
         layer_kernel,
@@ -801,15 +805,10 @@
             pltpu.VMEM((4, tokens, model), kind),
             pltpu.VMEM((4, tokens, model), kind),
             pltpu.VMEM(residual.shape, jnp.float32),
-            dma((12,)),
-            dma((2,)), dma((2,)),
-            dma((12,)), dma((12,)),
-            dma((3,)), dma((3,)),
-            dma((7,)), dma((7,)),
-            dma((6,)), dma((6,)),
-            dma((7, 2)), dma((4, 2)),
-            dma((4, 8)), dma((4, 8)), two, two, two, two, dma((7, 6)), dma((7, 6)),
-            dma((7, 2)), dma((7, 2)), dma((3,)), dma((3,)),
+            dma((12,)), dma((24,)),
+            dma((2,)), dma((2,)), dma((12,)), dma((3,)), dma((7,)), dma((6,)),
+            dma((7, 2)), dma((4, 2)), dma((3, 5)), dma((4,)), dma((4, 2)),
+            dma((7, 6)), dma((7, 2)), dma(()),
         ],
         compiler_params=pltpu.CompilerParams(
             collective_id=0, has_side_effects=True, vmem_limit_bytes=60 * 1024 * 1024

time: 87.8 us -> 86.6 us (0.986)
  Pallas kernels: 87 us -> 85.7 us
    pallas_call x1, Pallas kernels: 87 us -> 85.7 us  [layer(): pl.pallas_call(layer_kernel, out_shape=pltpu.VMEM(residual.shape, kind),...]
where the time goes in v6:
time: 86.6 us; the launch traced here: 86.4 us
  Pallas kernels  85.7 us (99%)
    pallas_call x1, Pallas kernels, layer(): pl.pallas_call(layer_kernel, out_shape=pltpu.VMEM(residual.shape, kind),...  85.7 us

profile of v6, /device:TPU:0, one launch (start us, length us, event | category | flops | bytes accessed | tf_op | source)
XLA Modules:
  0.0 86.4 jit_solution(8633028466995526766)
XLA Ops:
  0.0 85.7 %shard_map.118 = bf16[64,2048]{1,0:T(8,128)(2,1)S(1)} custom-call(bf16[256,512]{1,0:T(8,128)(2,1)} %q_hbm.1, bf16[256,256]{1,0:T(8,128)(2,1)} %k_hbm.1, bf16[256,256]{1,0:T(8,128)(2,1)} %v_hbm.1, f32[8]{0:T(128)} %sink_hbm.1, bf16[2048,512]{1,0:T(8,128)(2,1)} %w_hbm.1, bf16[64,2048]{1,0:T(8,128)(2,1)} %res_hbm.1, f32[1,2048]{1,0:T(1,128)} %bitcast.9, ...), custom_call_target="tpu_custom_call" | custom-call | tf_op jit(solution)/shard_map/pallas_call | solution.py:765
  85.7 0.7 copy.14

commit v7 on v6

--- a/solution.py
+++ b/solution.py
@@ -529,7 +529,7 @@
             rt[m, ty, low, columns], bx1[m, 1, :, columns]
         ).astype(mid.dtype)
         to_side = go(
-            mid.at[m, 0, :, columns], by2.at[m, :, columns], 16 + m, rr.at[k, 4], y_dev
+            mid.at[m, 0, :, columns], by2.at[m, :, columns], 16 + m, rr.at[k, 2], y_dev
         )
         firsts[m, c][1].wait_recv()
         mid[m, 1, :, columns] = wide_sum(
@@ -537,7 +537,7 @@
         ).astype(mid.dtype)
         seconds[m, c] = (
             to_side,
-            go(mid.at[m, 1, :, columns], bx2.at[m, :, columns], 16 + m, rr.at[k, 5], x_dev),
+            go(mid.at[m, 1, :, columns], bx2.at[m, :, columns], 16 + m, rr.at[k, 3], x_dev),
         )
 
     home_two = (jnp.where(inner, z_devs[2][0], z_devs[1][0]), t)
@@ -569,15 +569,14 @@
                 20 + m, zbr.at[k, h], home_two if m == 2 else z_devs[m],
             )
 
-        firsts[m, c][2].wait_recv()
-        seconds[m, c][0].wait_recv()
+        whole = rt.at[m, t, :, columns]
+        remote(whole, whole, sends.at[16 + m], rr.at[k, 2], x_dev).wait_recv()
         lower = home(
             low,
             wide_sum(rt[m, t, low, columns], bx1[m, 0, :, columns], by2[m, :, columns]),
             0,
         )
-        firsts[m, c][3].wait_recv()
-        seconds[m, c][1].wait_recv()
+        remote(whole, whole, sends.at[16 + m], rr.at[k, 3], x_dev).wait_recv()
         upper = home(
             high,
             wide_sum(rt[m, t, high, columns], by1[m, 0, :, columns], bx2[m, :, columns]),
@@ -663,10 +662,11 @@
     picked(2)
     rise(2, 0, 2)
     forward(3, 0)
-    rise(2, 2, total_steps)
+    rise(2, 2, total_steps - 1)
     forward(3, 1)
     reduce_far(0, 0)
     reduce_far(0, 1)
+    rise(2, total_steps - 1, total_steps)
     fall(2)
     complete(3)
     inverse_copies[3].wait_recv()
@@ -808,7 +808,7 @@
             dma((12,)), dma((24,)),
             dma((2,)), dma((2,)), dma((12,)), dma((3,)), dma((7,)), dma((6,)),
             dma((7, 2)), dma((4, 2)), dma((3, 5)), dma((4,)), dma((4, 2)),
-            dma((7, 6)), dma((7, 2)), dma(()),
+            dma((7, 4)), dma((7, 2)), dma(()),
         ],
         compiler_params=pltpu.CompilerParams(
             collective_id=0, has_side_effects=True, vmem_limit_bytes=60 * 1024 * 1024

time: 86.6 us -> 85.7 us (0.990)
    pallas_call x1, Pallas kernels: 85.7 us -> 84.9 us  [layer(): pl.pallas_call(layer_kernel, out_shape=pltpu.VMEM(residual.shape, kind),...]
where the time goes in v7:
time: 85.7 us; the launch traced here: 85.6 us
  Pallas kernels  84.9 us (99%)
    pallas_call x1, Pallas kernels, layer(): pl.pallas_call(layer_kernel, out_shape=pltpu.VMEM(residual.shape, kind),...  84.9 us

profile of v7, /device:TPU:0, one launch (start us, length us, event | category | flops | bytes accessed | tf_op | source)
XLA Modules:
  0.0 85.6 jit_solution(2293083580437857658)
XLA Ops:
  0.0 84.9 %shard_map.118 = bf16[64,2048]{1,0:T(8,128)(2,1)S(1)} custom-call(bf16[256,512]{1,0:T(8,128)(2,1)} %q_hbm.1, bf16[256,256]{1,0:T(8,128)(2,1)} %k_hbm.1, bf16[256,256]{1,0:T(8,128)(2,1)} %v_hbm.1, f32[8]{0:T(128)} %sink_hbm.1, bf16[2048,512]{1,0:T(8,128)(2,1)} %w_hbm.1, bf16[64,2048]{1,0:T(8,128)(2,1)} %res_hbm.1, f32[1,2048]{1,0:T(1,128)} %bitcast.9, ...), custom_call_target="tpu_custom_call" | custom-call | tf_op jit(solution)/shard_map/pallas_call | solution.py:765
  84.9 0.7 copy.14
